TPU v7x, 128 devices: a whole 4x4x4 slice. The times are simulated.
128 devices in a mesh: sp: 16 (over z, y), tp: 8 (over x, core).
Axes of the slice: x: 4, y: 4, z: 4, core: 2. Of those that a mesh axis runs over, the one named last changes fastest.
Arguments:
- gate_branch: bfloat16 [12288, 1024], P('sp', 'tp'), may hold values from -6 to 6
- recur_input: bfloat16 [12288, 1024], P('sp', 'tp'), may hold values from -6 to 6
- doc_ids: int32 [12288], P('sp'), may hold values from 0 to 7, never falling along the last dimension, each value on 1 to 4608 neighbouring positions
- conv_taps: bfloat16 [4, 1024], P(None, 'tp'), may hold values from -3 to 3
- gate_map: bfloat16 [16, 64, 64], P('tp'), may hold values from -0.75 to 0.75
- input_map: bfloat16 [16, 64, 64], P('tp'), may hold values from -0.75 to 0.75
- decay_level: float32 [1024], P('tp'), may hold values from 4.8 to 12.3
- decay_extra: float32 [12288, 1024], P('sp', 'tp'), may hold values from -2.1 to -1.9e-05
- out_weight: bfloat16 [1024, 2048], P(None, 'tp'), may hold values from -0.7875 to 0.7875
- residual: bfloat16 [12288, 2048], P('sp', 'tp'), may hold values from -44 to 44
- mix_gain: float32 [2048], P('tp'), may hold values from 0.1 to 1.9
- pre_gain: float32 [2048], P('tp'), may hold values from 0.1 to 1.9
- ffn_gain: float32 [2048], P('tp'), may hold values from 0.1 to 1.9
- gate_weight: bfloat16 [2048, 5632], P('sp', 'tp'), may hold values from -0.125 to 0.125
- up_weight: bfloat16 [2048, 5632], P('sp', 'tp'), may hold values from -0.125 to 0.125
- down_weight: bfloat16 [5632, 2048], P('tp', 'sp'), may hold values from -0.33579113 to 0.33579113
Outputs:
- layer_out: bfloat16 [12288, 2048], P('sp', 'tp')
Inputs may be any that keep to these rules, and one draw needn't show every extreme that they name: `doc_ids`: document numbers start at 0 and never fall along the sequence; a document has 1 to 4608 positions, and one has exactly that many.
All inputs are finite; a program needn't handle non-finite values.
Results may differ from a plain program's by a relative error of at most 0.013.
Values may be sent and summed in bfloat16 or wider, within the bound.
A program may use at most 64 MiB of HBM per device.

v0:
```python
import math

import jax
import jax.numpy as jnp
from jax import lax
from jax.sharding import Mesh
from jax.sharding import PartitionSpec as P

D = 2048
TP = ("tp_0", "tp_1")


epsilon = 1e-06
gate_power = 8.0


def in_one_piece(arrays, axis, dim, along):
    both = jnp.concatenate(arrays, axis=along)
    out, at, finished = (lax.all_gather(both, axis, axis=dim, tiled=True), 0, [])
    for a in arrays:
        finished.append(lax.slice_in_dim(out, at, at + a.shape[along], axis=along))
        at += a.shape[along]
    return tuple(finished)


def passed_along(block, axis, distance):
    devices = range(lax.axis_size(axis))
    route = [(i - distance, i) for i in devices if i - distance in devices]
    return lax.ppermute(block, axis, route)


def from_everyone(shard, axis):
    count = lax.axis_size(axis)
    return lax.all_to_all(
        jnp.broadcast_to(shard[None], (count, *shard.shape)), axis, 0, 0, tiled=True
    )


def collected_together(shard, axis):
    leaves = jax.tree.leaves(shard)
    order = sorted(range(len(leaves)), key=lambda k: -leaves[k].size)
    width = (1, *leaves[order[0]].shape)[-1]
    lines = [
        jnp.pad(leaves[k].reshape(-1), (0, -leaves[k].size % width)).reshape(-1, width)
        for k in order
    ]
    both, at, found = (from_everyone(jnp.concatenate(lines), axis), 0, {})
    for k, line in zip(order, lines):
        share = both[:, at : at + len(line)].reshape(len(both), -1)
        found[k] = share[:, : leaves[k].size].reshape(-1, *leaves[k].shape)
        at += len(line)
    numbers = iter(range(len(leaves)))
    return jax.tree.map(lambda _: found[next(numbers)], shard)


def combined_pairwise(pieces, combine):
    while len(jax.tree.leaves(pieces)[0]) > 1:
        pieces = jax.vmap(combine)(
            *(jax.tree.map(lambda part: part[side::2], pieces) for side in (0, 1))
        )
    return jax.tree.map(lambda part: part[0], pieces)


def carried_in(shard, axis, combine, identity):
    count, here = (lax.axis_size(axis), lax.axis_index(axis))
    passed = jnp.arange(count) < here

    def kept(part, zero, own):
        part = jnp.where(
            passed.reshape(-1, *(1 for _ in own.shape)), part, jnp.asarray(zero, own.dtype)
        )
        return part

    pieces = collected_together(shard, axis)
    return combined_pairwise(jax.tree.map(kept, pieces, identity, shard), combine)


def joined_along(blocks, dim):
    blocks = jnp.moveaxis(blocks, 0, dim)
    shape = blocks.shape
    return blocks.reshape(*shape[:dim], shape[dim] * shape[dim + 1], *shape[dim + 2 :])


def gathered_by_axis(shard, axes, dim):
    far, near = axes
    blocks = from_everyone(from_everyone(shard, far), near)
    return joined_along(blocks.swapaxes(0, 1).reshape(-1, *shard.shape), dim)


def taken_together(shard, axis):
    everything = from_everyone(shard, axis)
    return jnp.sum(everything, axis=0)


def combine(earlier, latter):
    return (earlier[0] * latter[0], latter[0] * earlier[1] + latter[1])


def block_recurrence(log_decay, driven, doc_ids, before_ids):
    tok_rows, local_width = log_decay.shape
    block_rows = math.gcd(tok_rows, 128)
    block_count = tok_rows // block_rows
    log_blocks = log_decay.reshape(block_count, block_rows, local_width)
    drive_blocks = driven.reshape(block_count, block_rows, local_width)
    id_blocks = doc_ids.reshape(block_count, block_rows)
    lower = jnp.arange(block_rows)[:, None] >= jnp.arange(block_rows)[None, :]

    def step(carry, pieces):
        prod_carry, state_carry = carry
        logs, drives, ids, before = pieces
        cumulative = jnp.cumsum(logs, axis=0)
        linked = jnp.logical_and(lower, ids[:, None] == ids[None, :])[:, :, None]
        spread = jnp.where(linked, cumulative[:, None, :] - cumulative[None, :, :], 0.0)
        weights = jnp.where(linked, jnp.exp(spread), 0.0)
        local = jnp.einsum("ijc,jc->ic", weights, drives)
        reach = jnp.exp(cumulative) * (ids == before).astype(jnp.float32)[:, None]
        block_states = local + reach * state_carry[None, :]
        block_prods = reach * prod_carry[None, :]
        return ((block_prods[-1], block_states[-1]), (block_prods, block_states))

    start = (jnp.ones((local_width,), jnp.float32), jnp.zeros((local_width,), jnp.float32))
    ends, outputs = lax.scan(step, start, (log_blocks, drive_blocks, id_blocks, before_ids))
    return (
        ends,
        outputs[0].reshape(tok_rows, local_width),
        outputs[1].reshape(tok_rows, local_width),
    )


def body(
    gate_branch,
    recur_input,
    doc_ids,
    conv_taps,
    gate_map,
    input_map,
    decay_level,
    decay_extra,
    out_weight,
    residual,
    mix_gain,
    pre_gain,
    ffn_gain,
    gate_weight,
    up_weight,
    down_weight,
):
    tok_rows, local_width = recur_input.shape
    reach_rows = conv_taps.shape[0] - 1
    head_size = gate_map.shape[1]
    gate_whole, up_whole = in_one_piece((gate_weight, up_weight), "sp", 0, 1)
    down_whole = lax.all_gather(down_weight, "sp", axis=1, tiled=True)
    rim_rows, rim_ids = passed_along(
        (recur_input[tok_rows - reach_rows :], doc_ids[tok_rows - reach_rows :]), "sp", 1
    )
    padded_ids = jnp.concatenate([rim_ids, doc_ids])
    padded_rows = jnp.concatenate([rim_rows, recur_input])
    tap_weights = conv_taps.astype(jnp.float32)
    convolved = recur_input.astype(jnp.float32) * tap_weights[0]
    for offset in range(1, reach_rows + 1):
        start_row = reach_rows - offset
        same_doc = (padded_ids[start_row : start_row + tok_rows] == doc_ids).astype(jnp.float32)[
            :, None
        ]
        convolved = (
            convolved
            + same_doc
            * padded_rows[start_row : start_row + tok_rows].astype(jnp.float32)
            * tap_weights[offset]
        )
    conv_out = convolved.astype(jnp.bfloat16)
    head_rows = conv_out.reshape(tok_rows, local_width // head_size, head_size)
    recur_gate = jax.nn.sigmoid(
        jnp.einsum("thd,hde->the", head_rows, gate_map, preferred_element_type=jnp.float32).reshape(
            tok_rows, local_width
        )
    )
    input_gate = jax.nn.sigmoid(
        jnp.einsum(
            "thd,hde->the", head_rows, input_map, preferred_element_type=jnp.float32
        ).reshape(tok_rows, local_width)
    )
    log_decay = gate_power * -jax.nn.softplus(-decay_level) * recur_gate + decay_extra
    driven = jnp.sqrt(-jnp.expm1(2.0 * log_decay)) * input_gate * conv_out.astype(jnp.float32)
    block_rows = math.gcd(tok_rows, 128)
    before_ids = padded_ids[reach_rows - 1 : reach_rows - 1 + tok_rows : block_rows]
    ends, products, states = block_recurrence(log_decay, driven, doc_ids, before_ids)
    identity = (jnp.ones((local_width,), jnp.float32), jnp.zeros((local_width,), jnp.float32))
    carried = carried_in(ends, "sp", combine, identity)
    states = states + products * carried[1][None, :]
    branch = (states * jax.nn.gelu(gate_branch.astype(jnp.float32))).astype(jnp.bfloat16)
    mixed_out = jnp.dot(
        gathered_by_axis(branch, ("tp_0", "tp_1"), 1),
        out_weight,
        preferred_element_type=jnp.float32,
    ).astype(jnp.bfloat16)
    mixed_f = mixed_out.astype(jnp.float32)
    mix_square = taken_together(jnp.sum(mixed_f * mixed_f, axis=1), TP)
    stream = (
        residual.astype(jnp.float32)
        + mixed_f * lax.rsqrt(mix_square / D + epsilon)[:, None] * mix_gain
    ).astype(jnp.bfloat16)
    stream_f = stream.astype(jnp.float32)
    pre_square = taken_together(jnp.sum(stream_f * stream_f, axis=1), TP)
    normed = (stream_f * lax.rsqrt(pre_square / D + epsilon)[:, None] * pre_gain).astype(
        jnp.bfloat16
    )
    whole_normed = gathered_by_axis(normed, ("tp_0", "tp_1"), 1)
    gate_act = jnp.dot(whole_normed, gate_whole, preferred_element_type=jnp.float32)
    up_act = jnp.dot(whole_normed, up_whole, preferred_element_type=jnp.float32)
    hidden = (jax.nn.silu(gate_act) * up_act).astype(jnp.bfloat16)
    partial_value = jnp.dot(hidden, down_whole, preferred_element_type=jnp.float32)
    ffn_out = lax.psum_scatter(
        partial_value.astype(jnp.bfloat16), TP, scatter_dimension=1, tiled=True
    )
    ffn_f = ffn_out.astype(jnp.float32)
    ffn_square = taken_together(jnp.sum(ffn_f * ffn_f, axis=1), TP)
    return (stream_f + ffn_f * lax.rsqrt(ffn_square / D + epsilon)[:, None] * ffn_gain).astype(
        jnp.bfloat16
    )


def solution(mesh):
    split = Mesh(mesh.devices.reshape(mesh.shape["sp"], 4, 2), ("sp", "tp_0", "tp_1"))
    return jax.shard_map(
        body,
        mesh=split,
        in_specs=(
            P("sp", TP),
            P("sp", TP),
            P("sp"),
            P(None, TP),
            P(TP, None, None),
            P(TP, None, None),
            P(TP),
            P("sp", TP),
            P(None, TP),
            P("sp", TP),
            P(TP),
            P(TP),
            P(TP),
            P("sp", TP),
            P("sp", TP),
            P(TP, "sp"),
        ),
        out_specs=P("sp", TP),
        check_vma=False,
    )
```

profile of v0, /device:TPU:1, one launch (start us, length us, event | category | flops | bytes accessed | tf_op | source)
XLA Modules:
  0.0 220.4 jit_solution(9097874307135880774)
XLA Ops:
  6.5 1.8 pad_maximum_fusion
  9.2 4.0 %collective-permute-start = (s32[3]{0:T(128)S(1)}, s32[3]{0:T(128)S(1)}, u32[]{:S(2)}, u32[]{:S(2)}) collective-permute-start(s32[3]{0:T(128)S(1)} %slice.106), channel_id=1, source_target_pairs={{0,8},{8,16},{16,24},{24,32},{32,40},{40,48},{48,56},{56,64},{64,7... | collective-permute-start | bytes 44 | tf_op jit(solution)/shard_map/ppermute | solution.py:29
  14.0 3.2 %collective-permute-start.1 = (bf16[3,128]{0,1:T(8,128)(2,1)S(1)}, bf16[3,128]{0,1:T(8,128)(2,1)S(1)}, u32[]{:S(2)}, u32[]{:S(2)}) collective-permute-start(bf16[3,128]{0,1:T(8,128)(2,1)S(1)} %copy.91), channel_id=1, source_target_pairs={{0,8},{8,16},{16,24},{24,32},{32,40},{40,48},{48,56},{56,64},{64,7... | collective-permute-start | bytes 2312 | tf_op jit(solution)/shard_map/ppermute | solution.py:29
  24.3 35.9 %while.17 = (s32[]{:T(128)}, f32[128]{0:T(128)S(1)}, f32[128]{0:T(128)S(1)}, f32[6,128,128]{2,1,0:T(8,128)S(1)}, f32[6,128,128]{2,1,0:T(8,128)S(1)}, /*index=5*/...) while((s32[]{:T(128)}, f32[128]{0:T(128)S(1)}, ...), condition=%wide.region_2.3_spmd.clone, body=%wide.region_0.2_spmd.clone.sunk | while | flops 12681602 | bytes 1023637 | solution.py:122
  25.0 1.3 compare_convert_fusion.2
  26.6 3.6 %multiply_reduce_fusion.3 = f32[128,128]{0,1:T(8,128)S(1)} fusion(f32[128,128]{0,1:T(8,128)S(1)} %get-tuple-element.205, f32[128,128]{1,0:T(8,128)S(1)} %reduce_window_sum.13, pred[128,128]{1,0:T(8,128)(4,1)S(1)} %fusion.63), kind=kLoop, calls=%fused_computation.1.clone.1 | loop fusion | flops 10469376 | bytes 212992 | tf_op jit(solution)/shard_map/while/body/eval_jaxpr/ijc,jc->ic/dot_general | solution.py:115
  30.9 1.3 compare_convert_fusion.2
  32.6 3.6 %multiply_reduce_fusion.3 = f32[128,128]{0,1:T(8,128)S(1)} fusion(f32[128,128]{0,1:T(8,128)S(1)} %get-tuple-element.205, f32[128,128]{1,0:T(8,128)S(1)} %reduce_window_sum.13, pred[128,128]{1,0:T(8,128)(4,1)S(1)} %fusion.63), kind=kLoop, calls=%fused_computation.1.clone.1 | loop fusion | flops 10469376 | bytes 212992 | tf_op jit(solution)/shard_map/while/body/eval_jaxpr/ijc,jc->ic/dot_general | solution.py:115
  36.9 1.3 compare_convert_fusion.2
  38.6 3.6 %multiply_reduce_fusion.3 = f32[128,128]{0,1:T(8,128)S(1)} fusion(f32[128,128]{0,1:T(8,128)S(1)} %get-tuple-element.205, f32[128,128]{1,0:T(8,128)S(1)} %reduce_window_sum.13, pred[128,128]{1,0:T(8,128)(4,1)S(1)} %fusion.63), kind=kLoop, calls=%fused_computation.1.clone.1 | loop fusion | flops 10469376 | bytes 212992 | tf_op jit(solution)/shard_map/while/body/eval_jaxpr/ijc,jc->ic/dot_general | solution.py:115
  42.9 1.3 compare_convert_fusion.2
  44.5 3.6 %multiply_reduce_fusion.3 = f32[128,128]{0,1:T(8,128)S(1)} fusion(f32[128,128]{0,1:T(8,128)S(1)} %get-tuple-element.205, f32[128,128]{1,0:T(8,128)S(1)} %reduce_window_sum.13, pred[128,128]{1,0:T(8,128)(4,1)S(1)} %fusion.63), kind=kLoop, calls=%fused_computation.1.clone.1 | loop fusion | flops 10469376 | bytes 212992 | tf_op jit(solution)/shard_map/while/body/eval_jaxpr/ijc,jc->ic/dot_general | solution.py:115
  48.9 1.3 compare_convert_fusion.2
  50.5 3.6 %multiply_reduce_fusion.3 = f32[128,128]{0,1:T(8,128)S(1)} fusion(f32[128,128]{0,1:T(8,128)S(1)} %get-tuple-element.205, f32[128,128]{1,0:T(8,128)S(1)} %reduce_window_sum.13, pred[128,128]{1,0:T(8,128)(4,1)S(1)} %fusion.63), kind=kLoop, calls=%fused_computation.1.clone.1 | loop fusion | flops 10469376 | bytes 212992 | tf_op jit(solution)/shard_map/while/body/eval_jaxpr/ijc,jc->ic/dot_general | solution.py:115
  56.5 3.6 %multiply_reduce_fusion.3 = f32[128,128]{0,1:T(8,128)S(1)} fusion(f32[128,128]{0,1:T(8,128)S(1)} %get-tuple-element.205, f32[128,128]{1,0:T(8,128)S(1)} %reduce_window_sum.13, pred[128,128]{1,0:T(8,128)(4,1)S(1)} %fusion.63), kind=kLoop, calls=%fused_computation.1.clone.1 | loop fusion | flops 10469376 | bytes 212992 | tf_op jit(solution)/shard_map/while/body/eval_jaxpr/ijc,jc->ic/dot_general | solution.py:115
  60.9 7.1 %all-to-all-start = ((f32[16,2,128]{2,1,0:T(2,128)}), f32[16,2,128]{2,1,0:T(2,128)S(1)}, u32[]{:S(2)}, u32[]{:S(2)}) async-start(f32[16,2,128]{2,1,0:T(2,128)} %broadcast_in_dim.64), calls=%async_computation | async-start | bytes 32768 | tf_op jit(solution)/shard_map/all_to_all | solution.py:34
  68.1 6.5 %all-to-all-done = f32[16,2,128]{2,1,0:T(2,128)S(1)} async-done(((f32[16,2,128]{2,1,0:T(2,128)}), f32[16,2,128]{2,1,0:T(2,128)S(1)}, u32[]{:S(2)}, u32[]{:S(2)}) %all-to-all-start) | async-done | bytes 16416 | tf_op jit(solution)/shard_map/all_to_all | solution.py:34
  75.2 13.1 %all_to_all.43 = bf16[4,768,128]{2,1,0:T(8,128)(2,1)S(1)} all-to-all(bf16[4,768,128]{2,1,0:T(8,128)(2,1)S(1)} %broadcast_in_dim.67), channel_id=1, replica_groups=mesh['sp'=16,'tp_0'=4,'tp_1'=2] {'tp_0'}, dimensions={0} | all-to-all | bytes 1572864 | tf_op jit(solution)/shard_map/all_to_all | solution.py:34
  88.5 8.6 %all_to_all.44 = bf16[2,4,768,128]{3,2,1,0:T(8,128)(2,1)S(1)} all-to-all(bf16[2,4,768,128]{3,2,1,0:T(8,128)(2,1)S(1)} %broadcast_in_dim.68), channel_id=1, replica_groups=mesh['sp'=16,'tp_0'=4,'tp_1'=2] {'tp_1'}, dimensions={0} | all-to-all | bytes 3145728 | tf_op jit(solution)/shard_map/all_to_all | solution.py:34
  97.2 1.6 copy.100
  98.8 2.1 multiply_reduce_fusion.1
  101.5 3.6 %all-to-all-start.3 = ((f32[8,1,768]{2,1,0:T(1,128)}), f32[8,1,768]{2,1,0:T(1,128)S(1)}, u32[]{:S(2)}, u32[]{:S(2)}) async-start(f32[8,1,768]{2,1,0:T(1,128)} %broadcast_in_dim.69), calls=%async_computation.3 | async-start | bytes 49152 | tf_op jit(solution)/shard_map/all_to_all | solution.py:34
  105.3 4.5 %all-to-all-done.3 = f32[8,1,768]{2,1,0:T(1,128)S(1)} async-done(((f32[8,1,768]{2,1,0:T(1,128)}), f32[8,1,768]{2,1,0:T(1,128)S(1)}, u32[]{:S(2)}, u32[]{:S(2)}) %all-to-all-start.3) | async-done | bytes 24608 | tf_op jit(solution)/shard_map/all_to_all | solution.py:34
  110.1 7.8 %all_to_all.45 = f32[8,1,768]{2,1,0:T(1,128)S(1)} all-to-all(f32[8,1,768]{2,1,0:T(1,128)S(1)} %broadcast_in_dim.70), channel_id=1, replica_groups=mesh['sp'=16,'tp_0'=4,'tp_1'=2] {'tp_0','tp_1'}, dimensions={0} | all-to-all | bytes 49152 | tf_op jit(solution)/shard_map/all_to_all | solution.py:34
  118.4 22.2 %all_to_all.46 = bf16[4,768,256]{2,1,0:T(8,128)(2,1)S(1)} all-to-all(bf16[4,768,256]{2,1,0:T(8,128)(2,1)S(1)} %broadcast_in_dim.71), channel_id=1, replica_groups=mesh['sp'=16,'tp_0'=4,'tp_1'=2] {'tp_0'}, dimensions={0} | all-to-all | bytes 3145728 | tf_op jit(solution)/shard_map/all_to_all | solution.py:34
  140.8 7.8 %all_to_all.47 = bf16[2,4,768,256]{3,2,1,0:T(8,128)(2,1)S(1)} all-to-all(bf16[2,4,768,256]{3,2,1,0:T(8,128)(2,1)S(1)} %broadcast_in_dim.72), channel_id=1, replica_groups=mesh['sp'=16,'tp_0'=4,'tp_1'=2] {'tp_1'}, dimensions={0} | all-to-all | bytes 6291456 | tf_op jit(solution)/shard_map/all_to_all | solution.py:34
  148.6 1.8 copy.104
  150.5 4.7 %copy.105 = bf16[768,8,256]{0,2,1:T(8,128)(2,1)} copy(bf16[768,8,256]{2,0,1:T(8,128)(2,1)} %bitcast.101) | data formatting | bytes 6291456 | tf_op jit(solution)/shard_map/transpose | solution.py:79
  155.2 5.2 %fusion.9 = f32[768,704]{0,1:T(8,128)S(1)} fusion(bf16[768,2048]{0,1:T(8,128)(2,1)} %bitcast.103, bf16[2048,1408]{0,1:T(8,128)(2,1)} %all-gather.3.cloned.1.call-done), kind=kOutput, calls=%fused_computation.21 | convolution fusion | flops 2214592512 | bytes 8192000 | tf_op jit(solution)/shard_map/dot_general | solution.py:209
  160.4 10.7 %convolution_convert_fusion = bf16[768,2048]{0,1:T(8,128)(2,1)} fusion(bf16[704,2048]{1,0:T(8,128)(2,1)} %all-gather.5.cloned.1.call-done, f32[768,704]{0,1:T(8,128)S(1)} %fusion.9, bf16[768,2048]{0,1:T(8,128)(2,1)} %bitcast.104, bf16[2048,1408]{0,1:T(8,128)(2,1)} %all-gather.3.cloned.1.call-done), kind=kOutput, calls=%fused_computation.18 | convolution fusion | flops 4434001920 | bytes 14221312 | tf_op jit(solution)/shard_map/dot_general | solution.py:212
  171.1 28.8 %reduce-scatter.2.cloned.1.call-done = bf16[768,256]{0,1:T(8,128)(2,1)} async-done(((bf16[768,2048]{0,1:T(8,128)(2,1)}), bf16[768,256]{0,1:T(8,128)(2,1)}) %reduce-scatter.2.cloned.1.call-update) | async-done | bytes 393232 | tf_op jit(solution)/shard_map/reduce_scatter | solution.py:213
  201.1 10.6 %all_to_all.48 = f32[8,1,768]{2,1,0:T(1,128)S(1)} all-to-all(f32[8,1,768]{2,1,0:T(1,128)S(1)} %broadcast_in_dim.73), channel_id=1, replica_groups=mesh['sp'=16,'tp_0'=4,'tp_1'=2] {'tp_0','tp_1'}, dimensions={0} | all-to-all | bytes 49152 | tf_op jit(solution)/shard_map/all_to_all | solution.py:34
  (139 shorter events, 22.5 us)
Async XLA Ops:
  6.5 92.3 %copy-start = (bf16[1024,256]{1,0:T(8,128)(2,1)S(1)}, bf16[1024,256]{1,0:T(8,128)(2,1)}, u32[]{:S(2)}) copy-start(bf16[1024,256]{1,0:T(8,128)(2,1)} %param.26) | copy-start | bytes 1572868
  6.5 16.4 %copy-start.6 = (bf16[2,64,64]{2,1,0:T(8,128)(2,1)S(1)}, bf16[2,64,64]{2,1,0:T(8,128)(2,1)}, u32[]{:S(2)}) copy-start(bf16[2,64,64]{2,1,0:T(8,128)(2,1)} %param.23) | copy-start | bytes 49156
  6.5 16.7 %copy-start.7 = (bf16[2,64,64]{2,1,0:T(8,128)(2,1)S(1)}, bf16[2,64,64]{2,1,0:T(8,128)(2,1)}, u32[]{:S(2)}) copy-start(bf16[2,64,64]{2,1,0:T(8,128)(2,1)} %param.22) | copy-start | bytes 49156
  6.5 148.7 %all-gather.3.cloned.1.call-start = ((), (), s32[]{:S(2)}) async-start(), calls=%async_computation.9 | async-start | bytes 6127616 | tf_op jit(solution)/shard_map/all_gather | solution.py:19
  8.4 152.0 %all-gather.5.cloned.1.call-start = ((), (), s32[]{:S(2)}) async-start(), calls=%async_computation.10 | async-start | bytes 3063808 | tf_op jit(solution)/shard_map/all_gather | solution.py:152
  9.2 11.7 %collective-permute-start = (s32[3]{0:T(128)S(1)}, s32[3]{0:T(128)S(1)}, u32[]{:S(2)}, u32[]{:S(2)}) collective-permute-start(s32[3]{0:T(128)S(1)} %slice.106), channel_id=1, source_target_pairs={{0,8},{8,16},{16,24},{24,32},{32,40},{40,48},{48,56},{56,64},{64,7... | collective-permute-start | bytes 44 | tf_op jit(solution)/shard_map/ppermute | solution.py:29
  14.0 8.5 %collective-permute-start.1 = (bf16[3,128]{0,1:T(8,128)(2,1)S(1)}, bf16[3,128]{0,1:T(8,128)(2,1)S(1)}, u32[]{:S(2)}, u32[]{:S(2)}) collective-permute-start(bf16[3,128]{0,1:T(8,128)(2,1)S(1)} %copy.91), channel_id=1, source_target_pairs={{0,8},{8,16},{16,24},{24,32},{32,40},{40,48},{48,56},{56,64},{64,7... | collective-permute-start | bytes 2312 | tf_op jit(solution)/shard_map/ppermute | solution.py:29
  24.3 50.6 %copy-start.2 = (bf16[768,128]{1,0:T(8,128)(2,1)S(1)}, bf16[768,128]{1,0:T(8,128)(2,1)}, u32[]{:S(2)}) copy-start(bf16[768,128]{1,0:T(8,128)(2,1)} %param.18) | copy-start | bytes 589828
  60.9 13.7 %all-to-all-start = ((f32[16,2,128]{2,1,0:T(2,128)}), f32[16,2,128]{2,1,0:T(2,128)S(1)}, u32[]{:S(2)}, u32[]{:S(2)}) async-start(f32[16,2,128]{2,1,0:T(2,128)} %broadcast_in_dim.64), calls=%async_computation | async-start | bytes 32768 | tf_op jit(solution)/shard_map/all_to_all | solution.py:34
  98.8 6.3 %copy-start.1 = (bf16[768,256]{1,0:T(8,128)(2,1)S(1)}, bf16[768,256]{1,0:T(8,128)(2,1)}, u32[]{:S(2)}) copy-start(bf16[768,256]{1,0:T(8,128)(2,1)} %param.27) | copy-start | bytes 1179652
  98.8 11.1 %copy-start.4 = (f32[256]{0:T(256)S(1)}, f32[256]{0:T(256)}, u32[]{:S(2)}) copy-start(f32[256]{0:T(256)} %param.28) | copy-start | bytes 3076
  98.8 19.1 %copy-start.3 = (f32[256]{0:T(256)S(1)}, f32[256]{0:T(256)}, u32[]{:S(2)}) copy-start(f32[256]{0:T(256)} %param.29) | copy-start | bytes 3076
  101.5 8.3 %all-to-all-start.3 = ((f32[8,1,768]{2,1,0:T(1,128)}), f32[8,1,768]{2,1,0:T(1,128)S(1)}, u32[]{:S(2)}, u32[]{:S(2)}) async-start(f32[8,1,768]{2,1,0:T(1,128)} %broadcast_in_dim.69), calls=%async_computation.3 | async-start | bytes 49152 | tf_op jit(solution)/shard_map/all_to_all | solution.py:34
  105.1 94.8 %reduce-scatter.2.cloned.1.call-start = ((), (), s32[]{:S(2)}) async-start(), calls=%async_computation.11 | async-start | bytes 3538944 | tf_op jit(solution)/shard_map/reduce_scatter | solution.py:213
  171.1 40.7 %copy-start.5 = (f32[256]{0:T(256)S(1)}, f32[256]{0:T(256)}, u32[]{:S(2)}) copy-start(f32[256]{0:T(256)} %param.30) | copy-start | bytes 3076
Sparse Core Ops, SparseCore 0:
  9.4 66.3 all-gather.2
  78.0 50.0 all-gather.4
  171.3 28.6 reduce-scatter.1
where the time goes:
time: 222 us; the launch traced here: 220 us
  blocking collectives  70.1 us (32%)
  other arithmetic  40.3 us (18%)
  waiting for transfers between devices  39.9 us (18%)
  local copies, waits for them, and re-layouts  19.7 us (9%)
  matrix products  18.6 us (8%)
  starting transfers between devices  18 us (8%)
  between operations  13.5 us (6%)
    all_to_all x6, blocking collectives, from_everyone(): lax.all_to_all(jnp.broadcast_to(shard[None], (count, *shard.shape)), axis...  70.1 us
    reduce_scatter x1, waiting for transfers between devices, body(): lax.psum_scatter(partial_value.astype(jnp.bfloat16), TP, scatter_dimensio...  28.8 us
    dot_general x6, other arithmetic, step(): local = jnp.einsum('ijc,jc->ic', weights, drives)  21.6 us
    all_to_all x2, waiting for transfers between devices, from_everyone(): lax.all_to_all(jnp.broadcast_to(shard[None], (count, *shard.shape)), axis...  11 us
    all_to_all x2, starting transfers between devices, from_everyone(): lax.all_to_all(jnp.broadcast_to(shard[None], (count, *shard.shape)), axis...  10.8 us
    dot_general x1, matrix products, body(): jnp.dot(hidden, down_whole, preferred_element_type=jnp.float32)  10.7 us
    convert_element_type x6, other arithmetic, step(): reach = jnp.exp(cumulative) * (ids == before).astype(jnp.float32)[:, None]  7.95 us
    ppermute x2, starting transfers between devices, passed_along(): return lax.ppermute(block, axis, route)  7.2 us
  transfers between devices with their start and end apart: 7, of which 3 were waited for; matrix products, arithmetic and copies ran while one was open for 28% of the time, Pallas kernels for 0%

commit v1 on v0

v1 whole, which is shorter than its diff:
```python
import jax
import jax.numpy as jnp
from jax import lax
from jax.experimental import pallas as pl
from jax.experimental.pallas import tpu as pltpu
from jax.sharding import PartitionSpec as P

MESH = pl.DeviceIdType.MESH
F32 = jnp.float32
BF16 = jnp.bfloat16

D = 2048
EPS = 1e-06
GATE_POWER = 8.0
TOK = 768
BLK = 96
HALF = 384
CH = 128
HID = 704
REACH = 6


def neg_expm1(u):
    series = 1.0 + u * (1.0 / 9.0)
    for n in (8.0, 7.0, 6.0, 5.0, 4.0, 3.0, 2.0):
        series = 1.0 + u * (1.0 / n) * series
    return jnp.where(u > -0.5, -u * series, 1.0 - jnp.exp(u))


def softplus(v):
    tail = jnp.exp(-jnp.abs(v))
    w = tail / (2.0 + tail)
    square = w * w
    series = jnp.full_like(w, 1.0 / 15.0)
    for n in (13.0, 11.0, 9.0, 7.0, 5.0, 3.0, 1.0):
        series = 1.0 / n + square * series
    return jnp.maximum(v, 0.0) + 2.0 * w * series


class TorusGather:
    def __init__(self, buf, rows, here, ring_send, ring_recv, pair_send, pair_recv):
        self.buf, self.rows = buf, rows
        self.z, self.y, self.c, self.t = here
        self.ring_send, self.ring_recv = ring_send, ring_recv
        self.pair_send, self.pair_recv = pair_send, pair_recv

    def slot(self, dz, dy):
        return lax.rem(self.z + dz, 4) * 4 + lax.rem(self.y + dy, 4)

    def at(self, half, a, b):
        return (a, b) if half == 0 else (b, a)

    def span(self, half, part):
        quarter = self.rows // 4
        first = half * 2 * quarter
        return (first, 2 * quarter) if part is None else (first + part * quarter, quarter)

    def piece(self, half, where, part=None):
        first, count = self.span(half, part)
        return self.buf.at[self.c, self.slot(*where), pl.ds(first, count)]

    def send(self, half, where, to, part=None):
        ref = self.piece(half, where, part)
        landed = ((where[0] - to[0]) % 4, (where[1] - to[1]) % 4)
        pltpu.make_async_remote_copy(
            src_ref=ref,
            dst_ref=ref,
            send_sem=self.ring_send,
            recv_sem=self.ring_recv.at[half, landed[0] * 4 + landed[1]],
            device_id=(self.slot(*to), self.t),
            device_id_type=MESH,
        ).start()

    def wait(self, half, where):
        ref = self.piece(half, where)
        pltpu.make_async_copy(ref, ref, self.ring_recv.at[half, where[0] * 4 + where[1]]).wait()
        self.pass_over(ref)

    def pass_over(self, ref):
        pltpu.make_async_remote_copy(
            src_ref=ref,
            dst_ref=ref,
            send_sem=self.pair_send,
            recv_sem=self.pair_recv,
            device_id=(self.slot(0, 0), self.t + 1 - 2 * self.c),
            device_id_type=MESH,
        ).start()

    def start(self):
        for first in (True, False):
            for half in (0, 1):
                for step in (1, 3):
                    to = self.at(half, 0, step) if first else self.at(half, step, 0)
                    self.send(half, (0, 0), to)
        self.pass_over(self.buf.at[self.c, self.slot(0, 0)])

    def spread(self, half, b):
        for step in (1, 3):
            self.send(half, self.at(half, 0, b), self.at(half, step, 0))

    def event(self, number):
        at = self.at
        for half in (0, 1):
            if number == 1:
                self.wait(half, at(half, 0, 3))
                self.send(half, at(half, 0, 3), at(half, 0, 1), part=0)
                self.wait(half, at(half, 0, 1))
                self.send(half, at(half, 0, 1), at(half, 0, 3), part=1)
        for half in (0, 1):
            if number == 1:
                self.spread(half, 3)
                self.spread(half, 1)
            if number == 2:
                self.wait(half, at(half, 0, 2))
                self.spread(half, 2)
            if number == 3:
                self.wait(half, at(half, 3, 0))
                self.send(half, at(half, 3, 0), at(half, 1, 0))
                self.wait(half, at(half, 1, 0))
            if number == 4:
                self.wait(half, at(half, 1, 3))
                self.send(half, at(half, 1, 3), at(half, 3, 0))
                self.wait(half, at(half, 3, 3))
            if number == 5:
                self.wait(half, at(half, 3, 1))
                self.send(half, at(half, 3, 1), at(half, 1, 0))
                self.wait(half, at(half, 1, 1))
            if number == 6:
                self.wait(half, at(half, 1, 2))
                self.send(half, at(half, 1, 2), at(half, 3, 0))
                self.wait(half, at(half, 3, 2))
            if number == 7:
                for b in (0, 3, 1, 2):
                    self.wait(half, at(half, 2, b))

    def wait_pair(self):
        ref = self.buf.at[1 - self.c]
        pltpu.make_async_copy(ref, ref, self.pair_recv).wait()

    def finish(self):
        ref = self.buf.at[self.c, pl.ds(0, 15)]
        pltpu.make_async_copy(ref, ref, self.ring_send).wait()
        ref = self.buf.at[self.c]
        pltpu.make_async_copy(ref, ref, self.pair_send).wait()


def layer_kernel(
    gate_ref, rec_ref, ids_ref, taps_ref, gmap_ref, imap_ref, level_ref, extra_ref, ow_ref, res_ref,
    mixg_ref, preg_ref, ffng_ref, gw_ref, uw_ref, dw_ref,
    out_ref,
    GU, DW, OW, BR, BRR, RB, GS, GB, HX, HI, XF, IDF, FA, DV, S, PR, GL, CS, CB, MX, ST, NB, H,
    PB, RA, RC, FO, SQS, SQB, XS, XR, PG,
    gu_ring, dw_ring, gu_sem, dw_sem, ow_ring, ow_sem, ag_ring, rs_recv, rs_send, sem,
):
    s, t = lax.axis_index("sp"), lax.axis_index("tp")
    z, y = lax.div(s, 4), lax.rem(s, 4)
    x, c = lax.div(t, 2), lax.rem(t, 2)
    mine = c * 4 + x

    def remote(src, dst, send_sem, recv_sem, device):
        copy = pltpu.make_async_remote_copy(
            src_ref=src, dst_ref=dst, send_sem=send_sem, recv_sem=recv_sem, device_id=device, device_id_type=MESH
        )
        copy.start()

    def await_bytes(ref, semaphore):
        pltpu.make_async_copy(ref, ref, semaphore).wait()

    def along_x(step):
        return (s, lax.rem(x + step, 4) * 2 + c)

    partner = (s, t + 1 - 2 * c)
    here = (z, y, c, t)
    gu = TorusGather(GU, 128, here, gu_sem.at[0], gu_ring, gu_sem.at[1], gu_sem.at[2])
    dw = TorusGather(DW, HID, here, dw_sem.at[0], dw_ring, dw_sem.at[1], dw_sem.at[2])

    barrier = pltpu.get_barrier_semaphore()
    for k in range(1, REACH + 1):
        for peer in (lax.rem(s + k, 16), lax.rem(s + 16 - k, 16)):
            pl.semaphore_signal(barrier, inc=1, device_id=(peer, t), device_id_type=MESH)
    for k in range(1, 8):
        pl.semaphore_signal(barrier, inc=1, device_id=(s, lax.rem(t + k, 8)), device_id_type=MESH)

    own = z * 4 + y
    for i in range(5):
        GU[c, own, :, 256 * i : 256 * i + 128] = gw_ref[:, 128 * i : 128 * i + 128]
        GU[c, own, :, 256 * i + 128 : 256 * i + 256] = uw_ref[:, 128 * i : 128 * i + 128]
    GU[c, own, :, 1280:1408] = jnp.concatenate([gw_ref[:, 640:704], uw_ref[:, 640:704]], axis=1)
    OW[c, x] = ow_ref[...]
    DW[c, own] = dw_ref[...]
    GS[...] = jnp.zeros_like(GS)
    GS[0:1] = mixg_ref[...]
    GS[1:2] = preg_ref[...]
    GS[2:3] = ffng_ref[...]
    GB[t] = GS[...]
    RB[t] = res_ref[mine]
    IDF[8:] = jnp.concatenate(
        [jnp.broadcast_to(ids_ref[r : r + 1, :].astype(F32), (128, 128)).T for r in range(6)], axis=0
    )
    XF[8:] = rec_ref[...].astype(F32)

    pl.semaphore_wait(barrier, 2 * REACH + 7)

    after = (lax.rem(s + 1, 16), t)
    remote(rec_ref.at[pl.ds(TOK - 16, 16)], HX, sem.at[0], sem.at[1], after)
    remote(ids_ref, HI, sem.at[2], sem.at[3], after)
    gu.start()
    for part, step in ((0, 1), (1, 3), (1, 1), (0, 3)):
        ref = OW.at[c, x, pl.ds(512 * part, 512)]
        remote(ref, ref, ow_sem.at[0], ow_ring.at[0 if step == 1 else 1, part], along_x(step))
    remote(OW.at[c, x], OW.at[c, x], ow_sem.at[1], ow_sem.at[2], partner)
    for k in range(1, 8):
        peer = lax.rem(t + k, 8)
        remote(GS, GB.at[t], sem.at[4], sem.at[5], (s, peer))
        block = lax.rem(peer, 2) * 4 + lax.div(peer, 2)
        remote(res_ref.at[block], RB.at[t], sem.at[6], sem.at[7], (s, peer))

    for r in range(6):
        rows = slice(128 * r, 128 * r + 128)
        GL[rows] = jax.nn.gelu(gate_ref[rows].astype(F32), approximate=True)
    pair = [
        jnp.concatenate(
            [
                jnp.concatenate([m[0].astype(F32), jnp.zeros((64, 64), F32)], axis=1),
                jnp.concatenate([jnp.zeros((64, 64), F32), m[1].astype(F32)], axis=1),
            ],
            axis=0,
        )
        for m in (gmap_ref, imap_ref)
    ]
    maps = jnp.concatenate(pair, axis=1).astype(BF16)
    rate = -GATE_POWER * softplus(-level_ref[...])
    taps = taps_ref[...].astype(F32)

    await_bytes(HX, sem.at[1])
    await_bytes(HI, sem.at[3])
    XF[0:8] = HX[...].astype(F32)[8:16]
    rim_ids = jnp.broadcast_to(HI[5:6, :].astype(F32), (128, 128)).T[120:128]
    IDF[0:8] = jnp.where(s > 0, rim_ids, -1.0)

    for r in range(6):
        at = 8 + 128 * r
        ids = IDF[at : at + 128]
        conv = XF[at : at + 128] * taps[0:1]
        for k in (1, 2, 3):
            same = IDF[at - k : at - k + 128] == ids
            conv = conv + jnp.where(same, XF[at - k : at - k + 128], 0.0) * taps[k : k + 1]
        conv = conv.astype(BF16)
        gates = jax.nn.sigmoid(jnp.dot(conv, maps, preferred_element_type=F32))
        rows = slice(128 * r, 128 * r + 128)
        log_decay = rate * gates[:, :CH] + extra_ref[rows]
        FA[rows] = jnp.where(IDF[at - 1 : at + 127] == ids, jnp.exp(log_decay), 0.0)
        DV[rows] = jnp.sqrt(neg_expm1(2.0 * log_decay)) * gates[:, CH:] * conv.astype(F32)

    state = jnp.zeros((8, CH), F32)
    prod = jnp.ones((8, CH), F32)
    for i in range(BLK):
        at = pl.ds(i, 8, stride=BLK)
        f = FA[at, :]
        state = f * state + DV[at, :]
        prod = f * prod
        S[at, :] = state
        PR[at, :] = prod
    befores = []
    p_all, e_all = jnp.ones((1, CH), F32), jnp.zeros((1, CH), F32)
    for b in range(8):
        befores.append((p_all, e_all))
        e_all = prod[b : b + 1] * e_all + state[b : b + 1]
        p_all = prod[b : b + 1] * p_all
    CS[...] = jnp.concatenate([p_all, e_all, jnp.zeros((6, CH), F32)], axis=0)
    gu.event(1)
    for k in range(1, REACH + 1):
        remote(CS, CB.at[k - 1], sem.at[8], sem.at[9], (lax.rem(s + k, 16), t))

    def ow_event(number):
        if number == 0:
            for part, step in ((0, 1), (1, 3)):
                came = lax.rem(x + 4 - step, 4)
                ref = OW.at[c, came, pl.ds(512 * part, 512)]
                await_bytes(ref, ow_ring.at[0 if step == 1 else 1, part])
                remote(ref, ref, ow_sem.at[0], ow_ring.at[2, part], along_x(step))
                remote(ref, ref, ow_sem.at[1], ow_sem.at[2], partner)
        if number == 1:
            for part, step in ((1, 1), (0, 3)):
                came = lax.rem(x + 4 - step, 4)
                ref = OW.at[c, came, pl.ds(512 * part, 512)]
                await_bytes(ref, ow_ring.at[0 if step == 1 else 1, part])
                remote(ref, ref, ow_sem.at[1], ow_sem.at[2], partner)
        if number == 2:
            came = lax.rem(x + 2, 4)
            for part in (0, 1):
                ref = OW.at[c, came, pl.ds(512 * part, 512)]
                await_bytes(ref, ow_ring.at[2, part])
                remote(ref, ref, ow_sem.at[1], ow_sem.at[2], partner)

    ow_event(0)

    await_bytes(CB, sem.at[9])
    entering = jnp.zeros((1, CH), F32)
    for k in range(REACH, 0, -1):
        entering = jnp.where(s >= k, CB[k - 1, 0:1] * entering + CB[k - 1, 1:2], 0.0)
    for b in range(8):
        rows = slice(BLK * b, BLK * b + BLK)
        p_before, e_before = befores[b]
        states = S[rows] + PR[rows] * (e_before + p_before * entering)
        BR[b] = (states * GL[rows]).astype(BF16)
    BRR[t] = BR[mine]
    gu.event(2)
    for k in range(1, 8):
        peer = lax.rem(t + k, 8)
        block = lax.rem(peer, 2) * 4 + lax.div(peer, 2)
        remote(BR.at[block], BRR.at[t], sem.at[10], sem.at[11], (s, peer))
    gu.event(3)
    gu.event(4)
    ow_event(1)
    gu.event(5)
    dw.start()
    ow_event(2)

    await_bytes(GB.at[pl.ds(0, 7)], sem.at[5])
    await_bytes(RB.at[pl.ds(0, 7)], sem.at[7])
    await_bytes(BRR.at[pl.ds(0, 7)], sem.at[11])
    await_bytes(OW.at[1 - c], ow_sem.at[2])
    PG[...] = jnp.concatenate([GB[j, 1:2] for j in range(8)], axis=1)
    branch = jnp.concatenate([BRR[j] for j in range(8)], axis=1)
    square = jnp.zeros((BLK, 1), F32)
    for j in range(8):
        mixed = jnp.dot(branch, OW[j % 2, j // 2], preferred_element_type=F32).astype(BF16).astype(F32)
        square = square + jnp.sum(mixed * mixed, axis=1, keepdims=True)
        MX[:, 256 * j : 256 * j + 256] = mixed
    scale = lax.rsqrt(square * (1.0 / D) + EPS)
    for j in range(8):
        cols = slice(256 * j, 256 * j + 256)
        mixed = MX[:, cols] * scale * GB[j, 0:1]
        ST[x, :, cols] = (RB[j].astype(F32) + mixed).astype(BF16)

    for part, step in ((0, 1), (1, 3), (1, 1), (0, 3)):
        ref = ST.at[x, pl.ds(48 * part, 48)]
        remote(ref, ref, sem.at[12], ag_ring.at[0 if step == 1 else 1, part], along_x(step))
    gu.event(6)
    for part, step in ((0, 1), (1, 3)):
        came = lax.rem(x + 4 - step, 4)
        ref = ST.at[came, pl.ds(48 * part, 48)]
        await_bytes(ref, ag_ring.at[0 if step == 1 else 1, part])
        remote(ref, ref, sem.at[12], ag_ring.at[2, part], along_x(step))
    gu.event(7)
    gu.wait_pair()

    def feed_forward_in(blocks):
        rows = BLK * len(blocks)
        for n, q in enumerate(blocks):
            for r in range(0, BLK, 16):
                stream = ST[q, r : r + 16].astype(F32)
                total = jnp.sum(stream * stream, axis=1, keepdims=True)
                NB[n, r : r + 16] = (stream * lax.rsqrt(total * (1.0 / D) + EPS) * PG[...]).astype(BF16)

        def lhs():
            return NB[0 : len(blocks)].reshape(rows, D)

        def half(p, carry):
            for i in range(5):
                weights = GU[p, :, :, 256 * i : 256 * i + 256].reshape(D, 256)
                both = jnp.dot(lhs(), weights, preferred_element_type=F32)
                act = (jax.nn.silu(both[:, :128]) * both[:, 128:]).astype(BF16)
                for n, q in enumerate(blocks):
                    H[p, q, :, 128 * i : 128 * i + 128] = act[BLK * n : BLK * n + BLK]
            return carry

        lax.fori_loop(0, 2, half, 0)
        weights = jnp.concatenate([GU[p, :, :, 1280:1408].reshape(D, 128) for p in (0, 1)], axis=1)
        both = jnp.dot(lhs(), weights, preferred_element_type=F32)
        for p in (0, 1):
            tail = both[:, 128 * p : 128 * p + 128]
            act = (jax.nn.silu(tail[:, :64]) * tail[:, 64:]).astype(BF16)
            for n, q in enumerate(blocks):
                H[p, q, :, 640:704] = act[BLK * n : BLK * n + BLK]

    left, right, across = lax.rem(x + 3, 4), lax.rem(x + 1, 4), lax.rem(x + 2, 4)
    feed_forward_in([x])
    dw.event(1)
    for part, step in ((1, 1), (0, 3)):
        came = lax.rem(x + 4 - step, 4)
        await_bytes(ST.at[came, pl.ds(48 * part, 48)], ag_ring.at[0 if step == 1 else 1, part])
    dw.event(2)
    dw.event(3)
    feed_forward_in([left, right])
    dw.event(4)
    for part in (0, 1):
        await_bytes(ST.at[across, pl.ds(48 * part, 48)], ag_ring.at[2, part])
    feed_forward_in([across])
    dw.event(5)
    dw.event(6)
    dw.event(7)
    dw.wait_pair()

    def down(chip, h):
        total = None
        for p in (0, 1):
            weights = jnp.concatenate([DW[p, 4 * chip + 2 * h], DW[p, 4 * chip + 2 * h + 1]], axis=1)
            part = jnp.dot(H[p].reshape(HALF, HID), weights, preferred_element_type=F32)
            total = part if total is None else total + part
        return total

    for h, step in ((0, 1), (1, 3)):
        PB[h] = down(across, h).astype(BF16)
        remote(PB.at[h], RA.at[h], rs_send.at[h], rs_recv.at[h], along_x(step))
    for n, (chip, h, step) in enumerate(((right, 1, 1), (left, 0, 3))):
        PB[2 + n] = down(chip, h).astype(BF16)
        remote(PB.at[2 + n], RC.at[n], rs_send.at[2 + n], rs_recv.at[2 + n], along_x(step))
    FO[0] = down(right, 0)
    FO[1] = down(left, 1)
    for n, step in enumerate((1, 3)):
        await_bytes(RA.at[n], rs_recv.at[n])
        PB[4 + n] = (FO[n] + RA[n].astype(F32)).astype(BF16)
        remote(PB.at[4 + n], RC.at[2 + n], rs_send.at[4 + n], rs_recv.at[4 + n], along_x(step))
    for h in (0, 1):
        FO[h] = down(x, h)
    for n, h in ((0, 1), (1, 0)):
        await_bytes(RC.at[n], rs_recv.at[2 + n])
        FO[h] = FO[h] + RC[n].astype(F32)
    square = jnp.zeros((HALF, 1), F32)
    for n, h in ((0, 0), (1, 1)):
        await_bytes(RC.at[2 + n], rs_recv.at[4 + n])
        total = (FO[h] + RC[2 + n].astype(F32)).astype(BF16).astype(F32)
        FO[h] = total
        square = square + jnp.sum(total * total, axis=1, keepdims=True)

    SQS[...] = jnp.broadcast_to(square, (HALF, 128)).T[0:8]
    for step in (1, 2, 3):
        remote(SQS, SQB.at[step - 1], sem.at[13], sem.at[14], along_x(step))
    await_bytes(SQB, sem.at[14])
    square = SQS[0:1] + SQB[0, 0:1] + SQB[1, 0:1] + SQB[2, 0:1]
    scale = lax.rsqrt(square * (1.0 / D) + EPS)
    scale = jnp.broadcast_to(scale, (128, HALF)).T
    scale = jnp.concatenate([scale, scale], axis=1)
    for h in (0, 1):
        cols = pl.ds(pl.multiple_of(512 * x + 256 * h, 256), 256)
        stream = ST[:, :, cols].reshape(HALF, 256).astype(F32)
        XS[h] = (stream + FO[h] * scale * GB[2 * x + h, 2:3]).astype(BF16)
    remote(XS.at[1 - c], XR, sem.at[15], sem.at[16], partner)
    out_ref[c] = XS[c]

    gu.finish()
    dw.finish()
    await_bytes(HX, sem.at[0])
    await_bytes(HI, sem.at[2])
    await_bytes(GB.at[pl.ds(0, 7)], sem.at[4])
    await_bytes(RB.at[pl.ds(0, 7)], sem.at[6])
    await_bytes(CB, sem.at[8])
    await_bytes(BRR.at[pl.ds(0, 7)], sem.at[10])
    await_bytes(OW.at[c, pl.ds(0, 3)], ow_sem.at[0])
    await_bytes(OW.at[c], ow_sem.at[1])
    await_bytes(ST.at[pl.ds(0, 3)], sem.at[12])
    for n in range(6):
        await_bytes(PB.at[n], rs_send.at[n])
    await_bytes(SQB, sem.at[13])
    await_bytes(XS.at[0], sem.at[15])
    await_bytes(XR, sem.at[16])
    out_ref[1 - c] = XR[...]


def body(
    gate_branch, recur_input, doc_ids, conv_taps, gate_map, input_map, decay_level, decay_extra, out_weight,
    residual, mix_gain, pre_gain, ffn_gain, gate_weight, up_weight, down_weight,
):
    vmem = pl.BlockSpec(memory_space=pltpu.VMEM)
    dma = pltpu.SemaphoreType.DMA
    out = pl.pallas_call(
        layer_kernel,
        name="layer",
        out_shape=jax.ShapeDtypeStruct((2, HALF, 256), BF16),
        in_specs=[vmem] * 16,
        out_specs=vmem,
        scratch_shapes=[
            pltpu.VMEM((2, 16, 128, 1408), BF16),
            pltpu.VMEM((2, 16, HID, 128), BF16),
            pltpu.VMEM((2, 4, 1024, 256), BF16),
            pltpu.VMEM((8, BLK, CH), BF16),
            pltpu.VMEM((8, BLK, CH), BF16),
            pltpu.VMEM((8, BLK, 256), BF16),
            pltpu.VMEM((8, 256), F32),
            pltpu.VMEM((8, 8, 256), F32),
            pltpu.VMEM((16, CH), BF16),
            pltpu.VMEM((6, 128), jnp.int32),
            pltpu.VMEM((TOK + 8, CH), F32),
            pltpu.VMEM((TOK + 8, CH), F32),
            pltpu.VMEM((TOK, CH), F32),
            pltpu.VMEM((TOK, CH), F32),
            pltpu.VMEM((TOK, CH), F32),
            pltpu.VMEM((TOK, CH), F32),
            pltpu.VMEM((TOK, CH), F32),
            pltpu.VMEM((8, CH), F32),
            pltpu.VMEM((REACH, 8, CH), F32),
            pltpu.VMEM((BLK, D), F32),
            pltpu.VMEM((4, BLK, D), BF16),
            pltpu.VMEM((2, BLK, D), BF16),
            pltpu.VMEM((2, 4, BLK, HID), BF16),
            pltpu.VMEM((6, HALF, 256), BF16),
            pltpu.VMEM((2, HALF, 256), BF16),
            pltpu.VMEM((4, HALF, 256), BF16),
            pltpu.VMEM((2, HALF, 256), F32),
            pltpu.VMEM((8, HALF), F32),
            pltpu.VMEM((3, 8, HALF), F32),
            pltpu.VMEM((2, HALF, 256), BF16),
            pltpu.VMEM((HALF, 256), BF16),
            pltpu.VMEM((1, D), F32),
            dma((2, 16)),
            dma((2, 16)),
            dma((3,)),
            dma((3,)),
            dma((3, 2)),
            dma((3,)),
            dma((3, 2)),
            dma((6,)),
            dma((6,)),
            dma((17,)),
        ],
        compiler_params=pltpu.CompilerParams(
            collective_id=0, has_side_effects=True, vmem_limit_bytes=60 * 1024 * 1024
        ),
    )(
        gate_branch,
        recur_input,
        doc_ids.reshape(6, 128),
        conv_taps,
        gate_map,
        input_map,
        decay_level.reshape(1, CH),
        decay_extra,
        out_weight,
        residual.reshape(8, BLK, 256),
        mix_gain.reshape(1, 256),
        pre_gain.reshape(1, 256),
        ffn_gain.reshape(1, 256),
        gate_weight,
        up_weight,
        down_weight,
    )
    return out.reshape(TOK, 256)


def solution(mesh):
    return jax.shard_map(
        body,
        mesh=mesh,
        in_specs=(
            P("sp", "tp"),
            P("sp", "tp"),
            P("sp"),
            P(None, "tp"),
            P("tp", None, None),
            P("tp", None, None),
            P("tp"),
            P("sp", "tp"),
            P(None, "tp"),
            P("sp", "tp"),
            P("tp"),
            P("tp"),
            P("tp"),
            P("sp", "tp"),
            P("sp", "tp"),
            P("tp", "sp"),
        ),
        out_specs=P("sp", "tp"),
        check_vma=False,
    )
```

time: 222 us -> 94.5 us (0.43)
  Pallas kernels: 0 us -> 90 us
  blocking collectives: 70.1 us -> 0 us
  other arithmetic: 40.3 us -> 0 us
  waiting for transfers between devices: 39.9 us -> 0 us
  matrix products: 18.6 us -> 0 us
  starting transfers between devices: 18 us -> 0 us
  local copies, waits for them, and re-layouts: 19.7 us -> 4.37 us
  between operations: 13.5 us -> 0.01 us
    pallas_call x0 -> x1, Pallas kernels: none -> 90 us  [body(): pl.pallas_call(layer_kernel, name='layer', out_shape=jax.ShapeDtypeStruct...]
    all_to_all x6 -> x0, blocking collectives: 70.1 us -> none  [from_everyone(): lax.all_to_all(jnp.broadcast_to(shard[None], (count, *shard.shape)), axis...]
    reduce_scatter x1 -> x0, waiting for transfers between devices: 28.8 us -> none  [body(): lax.psum_scatter(partial_value.astype(jnp.bfloat16), TP, scatter_dimensio...]
    dot_general x6 -> x0, other arithmetic: 21.6 us -> none  [step(): local = jnp.einsum('ijc,jc->ic', weights, drives)]
    dot_general x5 -> x0, matrix products: 18.6 us -> none  [the longest x1 10.7 us: body(): jnp.dot(hidden, down_whole, preferred_element_type=jnp.float32)]
    convert_element_type x12 -> x0, other arithmetic: 11.3 us -> none  [the longest x6 7.95 us: step(): reach = jnp.exp(cumulative) * (ids == before).astype(jnp.float32)[:, None]]
    all_to_all x2 -> x0, waiting for transfers between devices: 11 us -> none  [from_everyone(): lax.all_to_all(jnp.broadcast_to(shard[None], (count, *shard.shape)), axis...]
    all_to_all x2 -> x0, starting transfers between devices: 10.8 us -> none  [from_everyone(): lax.all_to_all(jnp.broadcast_to(shard[None], (count, *shard.shape)), axis...]
  transfers between devices with their start and end apart: 7 -> 0, of which waited for: 3 -> 0; matrix products, arithmetic and copies ran while one was open for 28% -> 0% of each run, Pallas kernels for 0% -> 0%
where the time goes in v1:
time: 94.5 us; the launch traced here: 94.3 us
  Pallas kernels  90 us (95%)
  local copies, waits for them, and re-layouts  4.37 us (5%)
    pallas_call x1, Pallas kernels, body(): pl.pallas_call(layer_kernel, name='layer', out_shape=jax.ShapeDtypeStruct...  90 us
    unnamed x5, local copies, waits for them, and re-layouts  4.37 us

profile of v1, /device:TPU:1, one launch (start us, length us, event | category | flops | bytes accessed | tf_op | source)
XLA Modules:
  0.0 94.3 jit_solution(1664764862816944047)
XLA Ops:
  0.0 0.0 copy-start
  0.0 1.8 %copy.17.gw_ref = bf16[128,704]{1,0:T(8,128)(2,1)} copy(bf16[128,704]{0,1:T(8,128)(2,1)} %param.29) | data formatting | bytes 360448 | tf_op args[13]
  1.8 0.0 copy-done
  1.8 0.8 copy.18.uw_ref
  2.6 90.0 %layer.1 = bf16[2,384,256]{2,1,0:T(8,128)(2,1)} custom-call(bf16[768,128]{1,0:T(8,128)(2,1)} %gate_ref.1, bf16[768,128]{1,0:T(8,128)(2,1)} %rec_ref.1, s32[6,128]{1,0:T(8,128)} %bitcast.9, bf16[4,128]{1,0:T(4,128)(2,1)} %taps_ref.1, bf16[2,64,64]{2,1,0:T(8,128)(2,1)} %gmap_ref.1, bf16[2,64,64]{2,1,0:T(8,128)(2,1)} %imap_ref.1, f32[1,128]{1,0:T(1,128)} %bitcast.13, ...), custom_call_target="tpu_custom_call" | custom-call | tf_op jit(solution)/shard_map/layer/pallas_call | solution.py:468
  92.6 1.8 %copy.20 = bf16[768,256]{1,0:T(8,128)(2,1)} copy(bf16[768,256]{1,0:T(8,128)(2,1)} %bitcast.7) | data formatting | bytes 786432
Async XLA Ops:
  0.0 1.8 %copy-start = (bf16[128,704]{0,1:T(8,128)(2,1)S(1)}, bf16[128,704]{0,1:T(8,128)(2,1)}, u32[]{:S(2)}) copy-start(bf16[128,704]{0,1:T(8,128)(2,1)} %param.30) | copy-start | bytes 540676

commit v2 on v1

--- a/solution.py
+++ b/solution.py
@@ -87,11 +87,14 @@
         ).start()
 
     def start(self):
-        for first in (True, False):
-            for half in (0, 1):
-                for step in (1, 3):
-                    to = self.at(half, 0, step) if first else self.at(half, step, 0)
-                    self.send(half, (0, 0), to)
+        for half in (0, 1):
+            for step in (1, 3):
+                self.send(half, (0, 0), self.at(half, 0, step))
+
+    def start_second(self):
+        for half in (0, 1):
+            for step in (1, 3):
+                self.send(half, (0, 0), self.at(half, step, 0))
         self.pass_over(self.buf.at[self.c, self.slot(0, 0)])
 
     def spread(self, half, b):
@@ -145,12 +148,14 @@
 
 
 def layer_kernel(
-    gate_ref, rec_ref, ids_ref, taps_ref, gmap_ref, imap_ref, level_ref, extra_ref, ow_ref, res_ref,
-    mixg_ref, preg_ref, ffng_ref, gw_ref, uw_ref, dw_ref,
+    gate_hbm, rec_hbm, ids_hbm, taps_hbm, gmap_hbm, imap_hbm, level_hbm, extra_hbm, ow_hbm, res_hbm,
+    mixg_hbm, preg_hbm, ffng_hbm, gw_hbm, uw_hbm, dw_hbm,
     out_ref,
+    gate_ref, rec_ref, ids_ref, taps_ref, gmap_ref, imap_ref, level_ref, extra_ref, res_ref,
+    mixg_ref, preg_ref, ffng_ref, gw_ref, uw_ref,
     GU, DW, OW, BR, BRR, RB, GS, GB, HX, HI, XF, IDF, FA, DV, S, PR, GL, CS, CB, MX, ST, NB, H,
-    PB, RA, RC, FO, SQS, SQB, XS, XR, PG,
-    gu_ring, dw_ring, gu_sem, dw_sem, ow_ring, ow_sem, ag_ring, rs_recv, rs_send, sem,
+    PB, RA, RC, PO, FO, SQB, XR, PG,
+    gu_ring, dw_ring, gu_sem, dw_sem, ow_ring, ow_sem, ag_ring, rs_recv, rs_send, in_sem, sem,
 ):
     s, t = lax.axis_index("sp"), lax.axis_index("tp")
     z, y = lax.div(s, 4), lax.rem(s, 4)
@@ -182,18 +187,31 @@
         pl.semaphore_signal(barrier, inc=1, device_id=(s, lax.rem(t + k, 8)), device_id_type=MESH)
 
     own = z * 4 + y
+    loads = []
+    for src, dst in (
+        (gw_hbm, gw_ref), (uw_hbm, uw_ref), (rec_hbm, rec_ref), (ids_hbm, ids_ref), (mixg_hbm, mixg_ref),
+        (preg_hbm, preg_ref), (ffng_hbm, ffng_ref), (ow_hbm, OW.at[c, x]), (gate_hbm, gate_ref), (taps_hbm, taps_ref),
+        (gmap_hbm, gmap_ref), (imap_hbm, imap_ref), (level_hbm, level_ref), (extra_hbm, extra_ref),
+        (res_hbm, res_ref), (dw_hbm, DW.at[c, own]),
+    ):
+        loads.append(pltpu.make_async_copy(src, dst, in_sem.at[len(loads)]))
+        loads[-1].start()
+
+    loads[0].wait()
+    loads[1].wait()
     for i in range(5):
-        GU[c, own, :, 256 * i : 256 * i + 128] = gw_ref[:, 128 * i : 128 * i + 128]
-        GU[c, own, :, 256 * i + 128 : 256 * i + 256] = uw_ref[:, 128 * i : 128 * i + 128]
-    GU[c, own, :, 1280:1408] = jnp.concatenate([gw_ref[:, 640:704], uw_ref[:, 640:704]], axis=1)
-    OW[c, x] = ow_ref[...]
-    DW[c, own] = dw_ref[...]
+        for n, ref in enumerate((gw_ref, uw_ref)):
+            block = ref[128 * i : 128 * i + 128].astype(F32).T.astype(BF16)
+            GU[c, own, :, 256 * i + 128 * n : 256 * i + 128 * n + 128] = block
+    block = jnp.concatenate([gw_ref[640:704].astype(F32), uw_ref[640:704].astype(F32)], axis=0)
+    GU[c, own, :, 1280:1408] = block.T.astype(BF16)
+    for load in loads[2:8]:
+        load.wait()
     GS[...] = jnp.zeros_like(GS)
     GS[0:1] = mixg_ref[...]
     GS[1:2] = preg_ref[...]
     GS[2:3] = ffng_ref[...]
     GB[t] = GS[...]
-    RB[t] = res_ref[mine]
     IDF[8:] = jnp.concatenate(
         [jnp.broadcast_to(ids_ref[r : r + 1, :].astype(F32), (128, 128)).T for r in range(6)], axis=0
     )
@@ -212,8 +230,9 @@
     for k in range(1, 8):
         peer = lax.rem(t + k, 8)
         remote(GS, GB.at[t], sem.at[4], sem.at[5], (s, peer))
-        block = lax.rem(peer, 2) * 4 + lax.div(peer, 2)
-        remote(res_ref.at[block], RB.at[t], sem.at[6], sem.at[7], (s, peer))
+    for load in loads[8:]:
+        load.wait()
+    RB[t] = res_ref[mine]
 
     for r in range(6):
         rows = slice(128 * r, 128 * r + 128)
@@ -268,9 +287,10 @@
         e_all = prod[b : b + 1] * e_all + state[b : b + 1]
         p_all = prod[b : b + 1] * p_all
     CS[...] = jnp.concatenate([p_all, e_all, jnp.zeros((6, CH), F32)], axis=0)
+    for k in range(1, REACH + 1):
+        remote(CS, CB.at[k - 1], sem.at[17], sem.at[9], (lax.rem(s + k, 16), t))
+    gu.start_second()
     gu.event(1)
-    for k in range(1, REACH + 1):
-        remote(CS, CB.at[k - 1], sem.at[8], sem.at[9], (lax.rem(s + k, 16), t))
 
     def ow_event(number):
         if number == 0:
@@ -305,20 +325,22 @@
         states = S[rows] + PR[rows] * (e_before + p_before * entering)
         BR[b] = (states * GL[rows]).astype(BF16)
     BRR[t] = BR[mine]
-    gu.event(2)
     for k in range(1, 8):
         peer = lax.rem(t + k, 8)
         block = lax.rem(peer, 2) * 4 + lax.div(peer, 2)
         remote(BR.at[block], BRR.at[t], sem.at[10], sem.at[11], (s, peer))
+    for k in range(1, 8):
+        peer = lax.rem(t + k, 8)
+        block = lax.rem(peer, 2) * 4 + lax.div(peer, 2)
+        remote(res_ref.at[block], RB.at[t], sem.at[6], sem.at[7], (s, peer))
+    gu.event(2)
     gu.event(3)
+    ow_event(1)
     gu.event(4)
-    ow_event(1)
+    ow_event(2)
     gu.event(5)
-    dw.start()
-    ow_event(2)
 
     await_bytes(GB.at[pl.ds(0, 7)], sem.at[5])
-    await_bytes(RB.at[pl.ds(0, 7)], sem.at[7])
     await_bytes(BRR.at[pl.ds(0, 7)], sem.at[11])
     await_bytes(OW.at[1 - c], ow_sem.at[2])
     PG[...] = jnp.concatenate([GB[j, 1:2] for j in range(8)], axis=1)
@@ -329,6 +351,10 @@
         square = square + jnp.sum(mixed * mixed, axis=1, keepdims=True)
         MX[:, 256 * j : 256 * j + 256] = mixed
     scale = lax.rsqrt(square * (1.0 / D) + EPS)
+    gu.event(6)
+    dw.start()
+    dw.start_second()
+    await_bytes(RB.at[pl.ds(0, 7)], sem.at[7])
     for j in range(8):
         cols = slice(256 * j, 256 * j + 256)
         mixed = MX[:, cols] * scale * GB[j, 0:1]
@@ -337,7 +363,6 @@
     for part, step in ((0, 1), (1, 3), (1, 1), (0, 3)):
         ref = ST.at[x, pl.ds(48 * part, 48)]
         remote(ref, ref, sem.at[12], ag_ring.at[0 if step == 1 else 1, part], along_x(step))
-    gu.event(6)
     for part, step in ((0, 1), (1, 3)):
         came = lax.rem(x + 4 - step, 4)
         ref = ST.at[came, pl.ds(48 * part, 48)]
@@ -346,29 +371,26 @@
     gu.event(7)
     gu.wait_pair()
 
-    def feed_forward_in(blocks):
-        rows = BLK * len(blocks)
+    def normalize(blocks):
         for n, q in enumerate(blocks):
             for r in range(0, BLK, 16):
                 stream = ST[q, r : r + 16].astype(F32)
                 total = jnp.sum(stream * stream, axis=1, keepdims=True)
                 NB[n, r : r + 16] = (stream * lax.rsqrt(total * (1.0 / D) + EPS) * PG[...]).astype(BF16)
 
-        def lhs():
-            return NB[0 : len(blocks)].reshape(rows, D)
-
-        def half(p, carry):
-            for i in range(5):
-                weights = GU[p, :, :, 256 * i : 256 * i + 256].reshape(D, 256)
-                both = jnp.dot(lhs(), weights, preferred_element_type=F32)
-                act = (jax.nn.silu(both[:, :128]) * both[:, 128:]).astype(BF16)
-                for n, q in enumerate(blocks):
-                    H[p, q, :, 128 * i : 128 * i + 128] = act[BLK * n : BLK * n + BLK]
-            return carry
-
-        lax.fori_loop(0, 2, half, 0)
+    def hidden(blocks, p):
+        lhs = NB[0 : len(blocks)].reshape(BLK * len(blocks), D)
+        for i in range(5):
+            weights = GU[p, :, :, 256 * i : 256 * i + 256].reshape(D, 256)
+            both = jnp.dot(lhs, weights, preferred_element_type=F32)
+            act = (jax.nn.silu(both[:, :128]) * both[:, 128:]).astype(BF16)
+            for n, q in enumerate(blocks):
+                H[p, q, :, 128 * i : 128 * i + 128] = act[BLK * n : BLK * n + BLK]
+
+    def hidden_tail(blocks):
+        lhs = NB[0 : len(blocks)].reshape(BLK * len(blocks), D)
         weights = jnp.concatenate([GU[p, :, :, 1280:1408].reshape(D, 128) for p in (0, 1)], axis=1)
-        both = jnp.dot(lhs(), weights, preferred_element_type=F32)
+        both = jnp.dot(lhs, weights, preferred_element_type=F32)
         for p in (0, 1):
             tail = both[:, 128 * p : 128 * p + 128]
             act = (jax.nn.silu(tail[:, :64]) * tail[:, 64:]).astype(BF16)
@@ -376,20 +398,31 @@
                 H[p, q, :, 640:704] = act[BLK * n : BLK * n + BLK]
 
     left, right, across = lax.rem(x + 3, 4), lax.rem(x + 1, 4), lax.rem(x + 2, 4)
-    feed_forward_in([x])
+    normalize([x])
+    hidden([x], 0)
     dw.event(1)
+    hidden([x], 1)
+    hidden_tail([x])
     for part, step in ((1, 1), (0, 3)):
         came = lax.rem(x + 4 - step, 4)
         await_bytes(ST.at[came, pl.ds(48 * part, 48)], ag_ring.at[0 if step == 1 else 1, part])
     dw.event(2)
     dw.event(3)
-    feed_forward_in([left, right])
+    normalize([left, right])
+    hidden([left, right], 0)
     dw.event(4)
+    hidden([left, right], 1)
+    hidden_tail([left, right])
     for part in (0, 1):
         await_bytes(ST.at[across, pl.ds(48 * part, 48)], ag_ring.at[2, part])
-    feed_forward_in([across])
+    theirs = pl.ds(pl.multiple_of(512 * x + 256 * (1 - c), 256), 256)
+    remote(ST.at[:, :, theirs], XR, sem.at[15], sem.at[16], partner)
     dw.event(5)
+    normalize([across])
+    hidden([across], 0)
     dw.event(6)
+    hidden([across], 1)
+    hidden_tail([across])
     dw.event(7)
     dw.wait_pair()
 
@@ -403,42 +436,48 @@
 
     for h, step in ((0, 1), (1, 3)):
         PB[h] = down(across, h).astype(BF16)
-        remote(PB.at[h], RA.at[h], rs_send.at[h], rs_recv.at[h], along_x(step))
-    for n, (chip, h, step) in enumerate(((right, 1, 1), (left, 0, 3))):
+        remote(PB.at[h], RA.at[h], rs_send.at[h], rs_recv.at[4 + h], along_x(step))
+    for n, (chip, h) in enumerate(((right, 1), (left, 0))):
         PB[2 + n] = down(chip, h).astype(BF16)
-        remote(PB.at[2 + n], RC.at[n], rs_send.at[2 + n], rs_recv.at[2 + n], along_x(step))
+        remote(PB.at[2 + n], RC.at[n, c], rs_send.at[2 + n], rs_recv.at[2 * n + c], (s, 2 * chip + h))
     FO[0] = down(right, 0)
     FO[1] = down(left, 1)
-    for n, step in enumerate((1, 3)):
-        await_bytes(RA.at[n], rs_recv.at[n])
+    for n, (chip, h) in enumerate(((right, 0), (left, 1))):
+        await_bytes(RA.at[n], rs_recv.at[4 + n])
         PB[4 + n] = (FO[n] + RA[n].astype(F32)).astype(BF16)
-        remote(PB.at[4 + n], RC.at[2 + n], rs_send.at[4 + n], rs_recv.at[4 + n], along_x(step))
-    for h in (0, 1):
-        FO[h] = down(x, h)
-    for n, h in ((0, 1), (1, 0)):
-        await_bytes(RC.at[n], rs_recv.at[2 + n])
-        FO[h] = FO[h] + RC[n].astype(F32)
-    square = jnp.zeros((HALF, 1), F32)
-    for n, h in ((0, 0), (1, 1)):
-        await_bytes(RC.at[2 + n], rs_recv.at[4 + n])
-        total = (FO[h] + RC[2 + n].astype(F32)).astype(BF16).astype(F32)
-        FO[h] = total
-        square = square + jnp.sum(total * total, axis=1, keepdims=True)
-
-    SQS[...] = jnp.broadcast_to(square, (HALF, 128)).T[0:8]
-    for step in (1, 2, 3):
-        remote(SQS, SQB.at[step - 1], sem.at[13], sem.at[14], along_x(step))
-    await_bytes(SQB, sem.at[14])
-    square = SQS[0:1] + SQB[0, 0:1] + SQB[1, 0:1] + SQB[2, 0:1]
+        remote(PB.at[4 + n], RC.at[n, c], rs_send.at[4 + n], rs_recv.at[2 * n + c], (s, 2 * chip + h))
+    PB[6] = down(x, 1 - c).astype(BF16)
+    remote(PB.at[6], PO.at[c], sem.at[8], sem.at[18], partner)
+    PO[c] = down(x, c).astype(BF16)
+    await_bytes(PO.at[0], sem.at[18])
+    for n in (0, 1):
+        for k in (0, 1):
+            await_bytes(RC.at[n, k], rs_recv.at[2 * n + k])
+    rows = []
+    for k in (0, 1):
+        total = PO[k].astype(F32) + RC[0, k].astype(F32) + RC[1, k].astype(F32)
+        total = total.astype(BF16).astype(F32)
+        FO[k] = total
+        square = jnp.sum(total * total, axis=1, keepdims=True)
+        rows.append(jnp.broadcast_to(square, (HALF, 128)).T[0:1])
+
+    SQB[t] = jnp.concatenate(rows, axis=1)
+    for k in range(1, 8):
+        remote(SQB.at[t], SQB.at[t], sem.at[13], sem.at[14], (s, lax.rem(t + k, 8)))
+    await_bytes(XR, sem.at[16])
+    await_bytes(SQB.at[pl.ds(0, 7)], sem.at[14])
+    square = SQB[0]
+    for j in range(1, 8):
+        square = square + SQB[j]
     scale = lax.rsqrt(square * (1.0 / D) + EPS)
-    scale = jnp.broadcast_to(scale, (128, HALF)).T
+    scale = jnp.broadcast_to(scale, (128, TOK)).T
     scale = jnp.concatenate([scale, scale], axis=1)
-    for h in (0, 1):
-        cols = pl.ds(pl.multiple_of(512 * x + 256 * h, 256), 256)
-        stream = ST[:, :, cols].reshape(HALF, 256).astype(F32)
-        XS[h] = (stream + FO[h] * scale * GB[2 * x + h, 2:3]).astype(BF16)
-    remote(XS.at[1 - c], XR, sem.at[15], sem.at[16], partner)
-    out_ref[c] = XS[c]
+    gain = GS[2:3]
+    mine_cols = pl.ds(pl.multiple_of(512 * x + 256 * c, 256), 256)
+    for k, stream in ((c, ST[:, :, mine_cols]), (1 - c, XR[...])):
+        stream = stream.reshape(HALF, 256).astype(F32)
+        factor = jnp.where(k == 0, scale[:HALF], scale[HALF:])
+        out_ref[k] = (stream + FO[k] * factor * gain).astype(BF16)
 
     gu.finish()
     dw.finish()
@@ -446,17 +485,16 @@
     await_bytes(HI, sem.at[2])
     await_bytes(GB.at[pl.ds(0, 7)], sem.at[4])
     await_bytes(RB.at[pl.ds(0, 7)], sem.at[6])
-    await_bytes(CB, sem.at[8])
+    await_bytes(CB, sem.at[17])
     await_bytes(BRR.at[pl.ds(0, 7)], sem.at[10])
     await_bytes(OW.at[c, pl.ds(0, 3)], ow_sem.at[0])
     await_bytes(OW.at[c], ow_sem.at[1])
     await_bytes(ST.at[pl.ds(0, 3)], sem.at[12])
     for n in range(6):
         await_bytes(PB.at[n], rs_send.at[n])
-    await_bytes(SQB, sem.at[13])
-    await_bytes(XS.at[0], sem.at[15])
-    await_bytes(XR, sem.at[16])
-    out_ref[1 - c] = XR[...]
+    await_bytes(PB.at[6], sem.at[8])
+    await_bytes(SQB.at[pl.ds(0, 7)], sem.at[13])
+    await_bytes(XR, sem.at[15])
 
 
 def body(
@@ -469,9 +507,23 @@
         layer_kernel,
         name="layer",
         out_shape=jax.ShapeDtypeStruct((2, HALF, 256), BF16),
-        in_specs=[vmem] * 16,
+        in_specs=[pl.BlockSpec(memory_space=pl.ANY)] * 16,
         out_specs=vmem,
         scratch_shapes=[
+            pltpu.VMEM((TOK, CH), BF16),
+            pltpu.VMEM((TOK, CH), BF16),
+            pltpu.VMEM((6, 128), jnp.int32),
+            pltpu.VMEM((4, CH), BF16),
+            pltpu.VMEM((2, 64, 64), BF16),
+            pltpu.VMEM((2, 64, 64), BF16),
+            pltpu.VMEM((1, CH), F32),
+            pltpu.VMEM((TOK, CH), F32),
+            pltpu.VMEM((8, BLK, 256), BF16),
+            pltpu.VMEM((1, 256), F32),
+            pltpu.VMEM((1, 256), F32),
+            pltpu.VMEM((1, 256), F32),
+            pltpu.VMEM((HID, 128), BF16),
+            pltpu.VMEM((HID, 128), BF16),
             pltpu.VMEM((2, 16, 128, 1408), BF16),
             pltpu.VMEM((2, 16, HID, 128), BF16),
             pltpu.VMEM((2, 4, 1024, 256), BF16),
@@ -495,14 +547,13 @@
             pltpu.VMEM((4, BLK, D), BF16),
             pltpu.VMEM((2, BLK, D), BF16),
             pltpu.VMEM((2, 4, BLK, HID), BF16),
-            pltpu.VMEM((6, HALF, 256), BF16),
+            pltpu.VMEM((7, HALF, 256), BF16),
             pltpu.VMEM((2, HALF, 256), BF16),
-            pltpu.VMEM((4, HALF, 256), BF16),
+            pltpu.VMEM((2, 2, HALF, 256), BF16),
+            pltpu.VMEM((2, HALF, 256), BF16),
             pltpu.VMEM((2, HALF, 256), F32),
-            pltpu.VMEM((8, HALF), F32),
-            pltpu.VMEM((3, 8, HALF), F32),
-            pltpu.VMEM((2, HALF, 256), BF16),
-            pltpu.VMEM((HALF, 256), BF16),
+            pltpu.VMEM((8, 1, TOK), F32),
+            pltpu.VMEM((4, BLK, 256), BF16),
             pltpu.VMEM((1, D), F32),
             dma((2, 16)),
             dma((2, 16)),
@@ -513,7 +564,8 @@
             dma((3, 2)),
             dma((6,)),
             dma((6,)),
-            dma((17,)),
+            dma((16,)),
+            dma((19,)),
         ],
         compiler_params=pltpu.CompilerParams(
             collective_id=0, has_side_effects=True, vmem_limit_bytes=60 * 1024 * 1024
@@ -532,8 +584,8 @@
         mix_gain.reshape(1, 256),
         pre_gain.reshape(1, 256),
         ffn_gain.reshape(1, 256),
-        gate_weight,
-        up_weight,
+        gate_weight.T,
+        up_weight.T,
         down_weight,
     )
     return out.reshape(TOK, 256)

time: 94.5 us -> 83.3 us (0.88)
  Pallas kernels: 90 us -> 81.4 us
  local copies, waits for them, and re-layouts: 4.37 us -> 1.77 us
    pallas_call x1, Pallas kernels: 90 us -> 81.4 us  [body(): pl.pallas_call(layer_kernel, name='layer', out_shape=jax.ShapeDtypeStruct...]
    unnamed x5 -> x1, local copies, waits for them, and re-layouts: 4.37 us -> 1.77 us
where the time goes in v2:
time: 83.3 us; the launch traced here: 83.1 us
  Pallas kernels  81.4 us (98%)
  local copies, waits for them, and re-layouts  1.77 us (2%)
    pallas_call x1, Pallas kernels, body(): pl.pallas_call(layer_kernel, name='layer', out_shape=jax.ShapeDtypeStruct...  81.4 us
    unnamed x1, local copies, waits for them, and re-layouts  1.77 us

profile of v2, /device:TPU:1, one launch (start us, length us, event | category | flops | bytes accessed | tf_op | source)
XLA Modules:
  0.0 83.1 jit_solution(1253526971042029297)
XLA Ops:
  0.0 81.4 %layer.1 = bf16[2,384,256]{2,1,0:T(8,128)(2,1)} custom-call(bf16[768,128]{1,0:T(8,128)(2,1)} %gate_hbm.1, bf16[768,128]{1,0:T(8,128)(2,1)} %rec_hbm.1, s32[6,128]{1,0:T(8,128)} %bitcast.13, bf16[4,128]{1,0:T(4,128)(2,1)} %taps_hbm.1, bf16[2,64,64]{2,1,0:T(8,128)(2,1)} %gmap_hbm.1, bf16[2,64,64]{2,1,0:T(8,128)(2,1)} %imap_hbm.1, f32[1,128]{1,0:T(1,128)} %bitcast.17, ...), custom_call_target="tpu_custom_call" | custom-call | tf_op jit(solution)/shard_map/layer/pallas_call | solution.py:506
  81.4 1.8 %copy.18 = bf16[768,256]{1,0:T(8,128)(2,1)} copy(bf16[768,256]{1,0:T(8,128)(2,1)} %bitcast.9) | data formatting | bytes 786432

commit v3 on v2

--- a/solution.py
+++ b/solution.py
@@ -133,8 +133,11 @@
                 self.send(half, at(half, 1, 2), at(half, 3, 0))
                 self.wait(half, at(half, 3, 2))
             if number == 7:
-                for b in (0, 3, 1, 2):
-                    self.wait(half, at(half, 2, b))
+                self.wait(half, at(half, 2, 0))
+                self.wait(half, at(half, 2, 3))
+            if number == 8:
+                self.wait(half, at(half, 2, 1))
+                self.wait(half, at(half, 2, 2))
 
     def wait_pair(self):
         ref = self.buf.at[1 - self.c]
@@ -363,13 +366,13 @@
     for part, step in ((0, 1), (1, 3), (1, 1), (0, 3)):
         ref = ST.at[x, pl.ds(48 * part, 48)]
         remote(ref, ref, sem.at[12], ag_ring.at[0 if step == 1 else 1, part], along_x(step))
+    gu.event(7)
     for part, step in ((0, 1), (1, 3)):
         came = lax.rem(x + 4 - step, 4)
         ref = ST.at[came, pl.ds(48 * part, 48)]
         await_bytes(ref, ag_ring.at[0 if step == 1 else 1, part])
         remote(ref, ref, sem.at[12], ag_ring.at[2, part], along_x(step))
-    gu.event(7)
-    gu.wait_pair()
+    gu.event(8)
 
     def normalize(blocks):
         for n, q in enumerate(blocks):
@@ -399,31 +402,33 @@
 
     left, right, across = lax.rem(x + 3, 4), lax.rem(x + 1, 4), lax.rem(x + 2, 4)
     normalize([x])
+    dw.event(1)
+    gu.wait_pair()
     hidden([x], 0)
-    dw.event(1)
+    dw.event(2)
+    dw.event(3)
     hidden([x], 1)
     hidden_tail([x])
     for part, step in ((1, 1), (0, 3)):
         came = lax.rem(x + 4 - step, 4)
         await_bytes(ST.at[came, pl.ds(48 * part, 48)], ag_ring.at[0 if step == 1 else 1, part])
-    dw.event(2)
-    dw.event(3)
+    dw.event(4)
     normalize([left, right])
     hidden([left, right], 0)
-    dw.event(4)
+    dw.event(5)
     hidden([left, right], 1)
     hidden_tail([left, right])
     for part in (0, 1):
         await_bytes(ST.at[across, pl.ds(48 * part, 48)], ag_ring.at[2, part])
     theirs = pl.ds(pl.multiple_of(512 * x + 256 * (1 - c), 256), 256)
     remote(ST.at[:, :, theirs], XR, sem.at[15], sem.at[16], partner)
-    dw.event(5)
+    dw.event(6)
     normalize([across])
     hidden([across], 0)
-    dw.event(6)
+    dw.event(7)
     hidden([across], 1)
     hidden_tail([across])
-    dw.event(7)
+    dw.event(8)
     dw.wait_pair()
 
     def down(chip, h):

time: 83.3 us -> 80 us (0.960)
  Pallas kernels: 81.4 us -> 78.1 us
    pallas_call x1, Pallas kernels: 81.4 us -> 78.1 us  [body(): pl.pallas_call(layer_kernel, name='layer', out_shape=jax.ShapeDtypeStruct...]
where the time goes in v3:
time: 80 us; the launch traced here: 79.8 us
  Pallas kernels  78.1 us (98%)
  local copies, waits for them, and re-layouts  1.77 us (2%)
    pallas_call x1, Pallas kernels, body(): pl.pallas_call(layer_kernel, name='layer', out_shape=jax.ShapeDtypeStruct...  78.1 us
    unnamed x1, local copies, waits for them, and re-layouts  1.77 us

profile of v3, /device:TPU:1, one launch (start us, length us, event | category | flops | bytes accessed | tf_op | source)
XLA Modules:
  0.0 79.8 jit_solution(11757940293893022829)
XLA Ops:
  0.0 78.1 %layer.1 = bf16[2,384,256]{2,1,0:T(8,128)(2,1)} custom-call(bf16[768,128]{1,0:T(8,128)(2,1)} %gate_hbm.1, bf16[768,128]{1,0:T(8,128)(2,1)} %rec_hbm.1, s32[6,128]{1,0:T(8,128)} %bitcast.13, bf16[4,128]{1,0:T(4,128)(2,1)} %taps_hbm.1, bf16[2,64,64]{2,1,0:T(8,128)(2,1)} %gmap_hbm.1, bf16[2,64,64]{2,1,0:T(8,128)(2,1)} %imap_hbm.1, f32[1,128]{1,0:T(1,128)} %bitcast.17, ...), custom_call_target="tpu_custom_call" | custom-call | tf_op jit(solution)/shard_map/layer/pallas_call | solution.py:511
  78.1 1.8 %copy.18 = bf16[768,256]{1,0:T(8,128)(2,1)} copy(bf16[768,256]{1,0:T(8,128)(2,1)} %bitcast.9) | data formatting | bytes 786432

commit v4 on v2

--- a/solution.py
+++ b/solution.py
@@ -74,14 +74,14 @@
     def wait(self, half, where):
         ref = self.piece(half, where)
         pltpu.make_async_copy(ref, ref, self.ring_recv.at[half, where[0] * 4 + where[1]]).wait()
-        self.pass_over(ref)
-
-    def pass_over(self, ref):
+        self.pass_over(ref, where)
+
+    def pass_over(self, ref, where):
         pltpu.make_async_remote_copy(
             src_ref=ref,
             dst_ref=ref,
             send_sem=self.pair_send,
-            recv_sem=self.pair_recv,
+            recv_sem=self.pair_recv.at[1 if where[1] == 2 else 0],
             device_id=(self.slot(0, 0), self.t + 1 - 2 * self.c),
             device_id_type=MESH,
         ).start()
@@ -95,50 +95,65 @@
         for half in (0, 1):
             for step in (1, 3):
                 self.send(half, (0, 0), self.at(half, step, 0))
-        self.pass_over(self.buf.at[self.c, self.slot(0, 0)])
-
-    def spread(self, half, b):
-        for step in (1, 3):
+        self.pass_over(self.buf.at[self.c, self.slot(0, 0)], (0, 0))
+
+    def spread(self, half, b, steps=(1, 3)):
+        for step in steps:
             self.send(half, self.at(half, 0, b), self.at(half, step, 0))
 
+    def relay(self, half, a, b):
+        self.wait(half, self.at(half, a, b))
+        self.send(half, self.at(half, a, b), self.at(half, 4 - a, 0))
+
     def event(self, number):
-        at = self.at
+        at, wait = self.at, self.wait
         for half in (0, 1):
             if number == 1:
-                self.wait(half, at(half, 0, 3))
+                wait(half, at(half, 0, 3))
                 self.send(half, at(half, 0, 3), at(half, 0, 1), part=0)
-                self.wait(half, at(half, 0, 1))
+                wait(half, at(half, 0, 1))
                 self.send(half, at(half, 0, 1), at(half, 0, 3), part=1)
         for half in (0, 1):
             if number == 1:
                 self.spread(half, 3)
                 self.spread(half, 1)
             if number == 2:
-                self.wait(half, at(half, 0, 2))
-                self.spread(half, 2)
+                if half == 0:
+                    self.relay(half, 3, 0)
+                    wait(half, at(half, 0, 2))
+                    self.spread(half, 2, (3,))
+                else:
+                    wait(half, at(half, 0, 2))
+                    self.spread(half, 2)
+                    self.relay(half, 3, 0)
+                wait(half, at(half, 1, 0))
             if number == 3:
-                self.wait(half, at(half, 3, 0))
-                self.send(half, at(half, 3, 0), at(half, 1, 0))
-                self.wait(half, at(half, 1, 0))
+                self.relay(half, 1, 3)
+                wait(half, at(half, 3, 3))
             if number == 4:
-                self.wait(half, at(half, 1, 3))
-                self.send(half, at(half, 1, 3), at(half, 3, 0))
-                self.wait(half, at(half, 3, 3))
-            if number == 5:
-                self.wait(half, at(half, 3, 1))
-                self.send(half, at(half, 3, 1), at(half, 1, 0))
-                self.wait(half, at(half, 1, 1))
-            if number == 6:
-                self.wait(half, at(half, 1, 2))
-                self.send(half, at(half, 1, 2), at(half, 3, 0))
-                self.wait(half, at(half, 3, 2))
-            if number == 7:
-                for b in (0, 3, 1, 2):
-                    self.wait(half, at(half, 2, b))
-
-    def wait_pair(self):
-        ref = self.buf.at[1 - self.c]
-        pltpu.make_async_copy(ref, ref, self.pair_recv).wait()
+                self.relay(half, 3, 1)
+                if half == 0:
+                    self.spread(half, 2, (1,))
+                wait(half, at(half, 1, 1))
+        if number == 5:
+            for half in (0, 1):
+                self.relay(half, 1, 2)
+            wait(1, at(1, 3, 2))
+        if number == 6:
+            wait(0, at(0, 2, 0))
+            wait(0, at(0, 2, 3))
+            wait(0, at(0, 2, 1))
+        if number == 7:
+            wait(1, at(1, 2, 0))
+            wait(1, at(1, 2, 3))
+            wait(0, at(0, 3, 2))
+            wait(0, at(0, 2, 2))
+            wait(1, at(1, 2, 1))
+            wait(1, at(1, 2, 2))
+
+    def wait_pair(self, late):
+        ref = self.buf.at[1 - self.c, pl.ds(0, 4 if late else 12)]
+        pltpu.make_async_copy(ref, ref, self.pair_recv.at[late]).wait()
 
     def finish(self):
         ref = self.buf.at[self.c, pl.ds(0, 15)]
@@ -154,8 +169,8 @@
     gate_ref, rec_ref, ids_ref, taps_ref, gmap_ref, imap_ref, level_ref, extra_ref, res_ref,
     mixg_ref, preg_ref, ffng_ref, gw_ref, uw_ref,
     GU, DW, OW, BR, BRR, RB, GS, GB, HX, HI, XF, IDF, FA, DV, S, PR, GL, CS, CB, MX, ST, NB, H,
-    PB, RA, RC, PO, FO, SQB, XR, PG,
-    gu_ring, dw_ring, gu_sem, dw_sem, ow_ring, ow_sem, ag_ring, rs_recv, rs_send, in_sem, sem,
+    PB, RA, RC, PO, FO, FF, SQB, XR, PG,
+    gu_ring, dw_ring, gu_sem, dw_sem, gu_pair, dw_pair, ow_ring, ow_sem, ag_ring, ra_recv, rc_recv, rs_send, in_sem, sem,
 ):
     s, t = lax.axis_index("sp"), lax.axis_index("tp")
     z, y = lax.div(s, 4), lax.rem(s, 4)
@@ -176,8 +191,8 @@
 
     partner = (s, t + 1 - 2 * c)
     here = (z, y, c, t)
-    gu = TorusGather(GU, 128, here, gu_sem.at[0], gu_ring, gu_sem.at[1], gu_sem.at[2])
-    dw = TorusGather(DW, HID, here, dw_sem.at[0], dw_ring, dw_sem.at[1], dw_sem.at[2])
+    gu = TorusGather(GU, 128, here, gu_sem.at[0], gu_ring, gu_sem.at[1], gu_pair)
+    dw = TorusGather(DW, HID, here, dw_sem.at[0], dw_ring, dw_sem.at[1], dw_pair)
 
     barrier = pltpu.get_barrier_semaphore()
     for k in range(1, REACH + 1):
@@ -334,11 +349,10 @@
         block = lax.rem(peer, 2) * 4 + lax.div(peer, 2)
         remote(res_ref.at[block], RB.at[t], sem.at[6], sem.at[7], (s, peer))
     gu.event(2)
+    ow_event(1)
     gu.event(3)
-    ow_event(1)
+    ow_event(2)
     gu.event(4)
-    ow_event(2)
-    gu.event(5)
 
     await_bytes(GB.at[pl.ds(0, 7)], sem.at[5])
     await_bytes(BRR.at[pl.ds(0, 7)], sem.at[11])
@@ -351,7 +365,7 @@
         square = square + jnp.sum(mixed * mixed, axis=1, keepdims=True)
         MX[:, 256 * j : 256 * j + 256] = mixed
     scale = lax.rsqrt(square * (1.0 / D) + EPS)
-    gu.event(6)
+    gu.event(5)
     dw.start()
     dw.start_second()
     await_bytes(RB.at[pl.ds(0, 7)], sem.at[7])
@@ -363,14 +377,13 @@
     for part, step in ((0, 1), (1, 3), (1, 1), (0, 3)):
         ref = ST.at[x, pl.ds(48 * part, 48)]
         remote(ref, ref, sem.at[12], ag_ring.at[0 if step == 1 else 1, part], along_x(step))
+    gu.event(6)
+    gu.event(7)
     for part, step in ((0, 1), (1, 3)):
         came = lax.rem(x + 4 - step, 4)
         ref = ST.at[came, pl.ds(48 * part, 48)]
         await_bytes(ref, ag_ring.at[0 if step == 1 else 1, part])
         remote(ref, ref, sem.at[12], ag_ring.at[2, part], along_x(step))
-    gu.event(7)
-    gu.wait_pair()
-
     def normalize(blocks):
         for n, q in enumerate(blocks):
             for r in range(0, BLK, 16):
@@ -399,69 +412,94 @@
 
     left, right, across = lax.rem(x + 3, 4), lax.rem(x + 1, 4), lax.rem(x + 2, 4)
     normalize([x])
+    dw.event(1)
+    gu.wait_pair(0)
+    gu.wait_pair(1)
     hidden([x], 0)
-    dw.event(1)
     hidden([x], 1)
     hidden_tail([x])
+    dw.event(2)
     for part, step in ((1, 1), (0, 3)):
         came = lax.rem(x + 4 - step, 4)
         await_bytes(ST.at[came, pl.ds(48 * part, 48)], ag_ring.at[0 if step == 1 else 1, part])
-    dw.event(2)
-    dw.event(3)
     normalize([left, right])
     hidden([left, right], 0)
-    dw.event(4)
+    dw.event(3)
     hidden([left, right], 1)
     hidden_tail([left, right])
+    dw.event(4)
     for part in (0, 1):
         await_bytes(ST.at[across, pl.ds(48 * part, 48)], ag_ring.at[2, part])
     theirs = pl.ds(pl.multiple_of(512 * x + 256 * (1 - c), 256), 256)
     remote(ST.at[:, :, theirs], XR, sem.at[15], sem.at[16], partner)
-    dw.event(5)
     normalize([across])
     hidden([across], 0)
-    dw.event(6)
+    dw.event(5)
     hidden([across], 1)
     hidden_tail([across])
+    dw.event(6)
+
+    def down_of(p, chip, h):
+        weights = jnp.concatenate([DW[p, 4 * chip + 2 * h], DW[p, 4 * chip + 2 * h + 1]], axis=1)
+        return jnp.dot(H[p].reshape(HALF, HID), weights, preferred_element_type=F32)
+
+    def down(chip, h):
+        return down_of(c, chip, h) + down_of(1 - c, chip, h)
+
+    QUARTER = HALF // 2
+    top, bottom = pl.ds(0, QUARTER), pl.ds(QUARTER, QUARTER)
+
+    def scatter_across(n, total):
+        PB[n, 0] = total.astype(BF16)
+        for m, (rows, step) in enumerate(((top, 1), (bottom, 3))):
+            remote(PB.at[n, 0, rows], RA.at[n, m], rs_send.at[n, m], ra_recv.at[n, m], along_x(step))
+
+    def scatter_near(n, h):
+        for m, (chip, rows) in enumerate(((right, bottom), (left, top))):
+            total = down(chip, h)
+            PB[n, 1 + m] = total.astype(BF16)
+            FO[n, m] = total[:QUARTER] if m == 0 else total[QUARTER:]
+            remote(
+                PB.at[n, 1 + m, rows], RC.at[m, c, rows], rs_send.at[n, 2 + m], rc_recv.at[m, c, 1 - m],
+                (s, 2 * chip + h),
+            )
+
+    def scatter_relay(n, h):
+        for m, (chip, rows) in enumerate(((right, top), (left, bottom))):
+            await_bytes(RA.at[n, m], ra_recv.at[n, m])
+            PB[n, 1 + m, rows] = (FO[n, m] + RA[n, m].astype(F32)).astype(BF16)
+            remote(
+                PB.at[n, 1 + m, rows], RC.at[m, c, rows], rs_send.at[n, 4 + m], rc_recv.at[m, c, m],
+                (s, 2 * chip + h),
+            )
+
+    early = lax.div(y, 2)
+    total = down_of(c, across, early)
+    dw.wait_pair(0)
+    scatter_across(0, total + down_of(1 - c, across, early))
     dw.event(7)
-    dw.wait_pair()
-
-    def down(chip, h):
-        total = None
-        for p in (0, 1):
-            weights = jnp.concatenate([DW[p, 4 * chip + 2 * h], DW[p, 4 * chip + 2 * h + 1]], axis=1)
-            part = jnp.dot(H[p].reshape(HALF, HID), weights, preferred_element_type=F32)
-            total = part if total is None else total + part
-        return total
-
-    for h, step in ((0, 1), (1, 3)):
-        PB[h] = down(across, h).astype(BF16)
-        remote(PB.at[h], RA.at[h], rs_send.at[h], rs_recv.at[4 + h], along_x(step))
-    for n, (chip, h) in enumerate(((right, 1), (left, 0))):
-        PB[2 + n] = down(chip, h).astype(BF16)
-        remote(PB.at[2 + n], RC.at[n, c], rs_send.at[2 + n], rs_recv.at[2 * n + c], (s, 2 * chip + h))
-    FO[0] = down(right, 0)
-    FO[1] = down(left, 1)
-    for n, (chip, h) in enumerate(((right, 0), (left, 1))):
-        await_bytes(RA.at[n], rs_recv.at[4 + n])
-        PB[4 + n] = (FO[n] + RA[n].astype(F32)).astype(BF16)
-        remote(PB.at[4 + n], RC.at[n, c], rs_send.at[4 + n], rs_recv.at[2 * n + c], (s, 2 * chip + h))
-    PB[6] = down(x, 1 - c).astype(BF16)
-    remote(PB.at[6], PO.at[c], sem.at[8], sem.at[18], partner)
+    scatter_near(0, early)
+    dw.wait_pair(1)
+    scatter_across(1, down(across, 1 - early))
+    scatter_relay(0, early)
+    scatter_near(1, 1 - early)
+    PB[0, 3] = down(x, 1 - c).astype(BF16)
+    remote(PB.at[0, 3], PO.at[c], sem.at[8], sem.at[18], partner)
+    scatter_relay(1, 1 - early)
     PO[c] = down(x, c).astype(BF16)
-    await_bytes(PO.at[0], sem.at[18])
-    for n in (0, 1):
-        for k in (0, 1):
-            await_bytes(RC.at[n, k], rs_recv.at[2 * n + k])
-    rows = []
+    await_bytes(PO.at[1 - c], sem.at[18])
+    sums = []
     for k in (0, 1):
+        for m in (0, 1):
+            for part, rows in ((0, top), (1, bottom)):
+                await_bytes(RC.at[m, k, rows], rc_recv.at[m, k, part])
         total = PO[k].astype(F32) + RC[0, k].astype(F32) + RC[1, k].astype(F32)
         total = total.astype(BF16).astype(F32)
-        FO[k] = total
+        FF[k] = total
         square = jnp.sum(total * total, axis=1, keepdims=True)
-        rows.append(jnp.broadcast_to(square, (HALF, 128)).T[0:1])
-
-    SQB[t] = jnp.concatenate(rows, axis=1)
+        sums.append(jnp.broadcast_to(square, (HALF, 128)).T[0:1])
+
+    SQB[t] = jnp.concatenate(sums, axis=1)
     for k in range(1, 8):
         remote(SQB.at[t], SQB.at[t], sem.at[13], sem.at[14], (s, lax.rem(t + k, 8)))
     await_bytes(XR, sem.at[16])
@@ -477,7 +515,7 @@
     for k, stream in ((c, ST[:, :, mine_cols]), (1 - c, XR[...])):
         stream = stream.reshape(HALF, 256).astype(F32)
         factor = jnp.where(k == 0, scale[:HALF], scale[HALF:])
-        out_ref[k] = (stream + FO[k] * factor * gain).astype(BF16)
+        out_ref[k] = (stream + FF[k] * factor * gain).astype(BF16)
 
     gu.finish()
     dw.finish()
@@ -490,9 +528,10 @@
     await_bytes(OW.at[c, pl.ds(0, 3)], ow_sem.at[0])
     await_bytes(OW.at[c], ow_sem.at[1])
     await_bytes(ST.at[pl.ds(0, 3)], sem.at[12])
-    for n in range(6):
-        await_bytes(PB.at[n], rs_send.at[n])
-    await_bytes(PB.at[6], sem.at[8])
+    for n in (0, 1):
+        for m in range(6):
+            await_bytes(PB.at[0, 0, top], rs_send.at[n, m])
+    await_bytes(PB.at[0, 3], sem.at[8])
     await_bytes(SQB.at[pl.ds(0, 7)], sem.at[13])
     await_bytes(XR, sem.at[15])
 
@@ -506,7 +545,7 @@
     out = pl.pallas_call(
         layer_kernel,
         name="layer",
-        out_shape=jax.ShapeDtypeStruct((2, HALF, 256), BF16),
+        out_shape=pltpu.VMEM((2, HALF, 256), BF16),
         in_specs=[pl.BlockSpec(memory_space=pl.ANY)] * 16,
         out_specs=vmem,
         scratch_shapes=[
@@ -547,23 +586,27 @@
             pltpu.VMEM((4, BLK, D), BF16),
             pltpu.VMEM((2, BLK, D), BF16),
             pltpu.VMEM((2, 4, BLK, HID), BF16),
-            pltpu.VMEM((7, HALF, 256), BF16),
-            pltpu.VMEM((2, HALF, 256), BF16),
+            pltpu.VMEM((2, 4, HALF, 256), BF16),
+            pltpu.VMEM((2, 2, HALF // 2, 256), BF16),
             pltpu.VMEM((2, 2, HALF, 256), BF16),
             pltpu.VMEM((2, HALF, 256), BF16),
+            pltpu.VMEM((2, 2, HALF // 2, 256), F32),
             pltpu.VMEM((2, HALF, 256), F32),
             pltpu.VMEM((8, 1, TOK), F32),
             pltpu.VMEM((4, BLK, 256), BF16),
             pltpu.VMEM((1, D), F32),
             dma((2, 16)),
             dma((2, 16)),
-            dma((3,)),
-            dma((3,)),
+            dma((2,)),
+            dma((2,)),
+            dma((2,)),
+            dma((2,)),
             dma((3, 2)),
             dma((3,)),
             dma((3, 2)),
-            dma((6,)),
-            dma((6,)),
+            dma((2, 2)),
+            dma((2, 2, 2)),
+            dma((2, 6)),
             dma((16,)),
             dma((19,)),
         ],

time: 83.3 us -> 76.7 us (0.921)
  Pallas kernels: 81.4 us -> 75.8 us
  local copies, waits for them, and re-layouts: 1.77 us -> 0.75 us
    pallas_call x1, Pallas kernels: 81.4 us -> 75.8 us  [body(): pl.pallas_call(layer_kernel, name='layer', out_shape=pltpu.VMEM((2, HALF,...]
    unnamed x1, local copies, waits for them, and re-layouts: 1.77 us -> 0.75 us
where the time goes in v4:
time: 76.7 us; the launch traced here: 76.6 us
  Pallas kernels  75.8 us (99%)
    pallas_call x1, Pallas kernels, body(): pl.pallas_call(layer_kernel, name='layer', out_shape=pltpu.VMEM((2, HALF,...  75.8 us

profile of v4, /device:TPU:1, one launch (start us, length us, event | category | flops | bytes accessed | tf_op | source)
XLA Modules:
  0.0 76.6 jit_solution(9779893190551190140)
XLA Ops:
  0.0 75.8 %layer.1 = bf16[2,384,256]{2,1,0:T(8,128)(2,1)S(1)} custom-call(bf16[768,128]{1,0:T(8,128)(2,1)} %gate_hbm.1, bf16[768,128]{1,0:T(8,128)(2,1)} %rec_hbm.1, s32[6,128]{1,0:T(8,128)} %bitcast.13, bf16[4,128]{1,0:T(4,128)(2,1)} %taps_hbm.1, bf16[2,64,64]{2,1,0:T(8,128)(2,1)} %gmap_hbm.1, bf16[2,64,64]{2,1,0:T(8,128)(2,1)} %imap_hbm.1, f32[1,128]{1,0:T(1,128)} %bitcast.17, ...), custom_call_target="tpu_custom_call" | custom-call | tf_op jit(solution)/shard_map/layer/pallas_call | solution.py:545
  75.8 0.7 copy.18

commit v5 on v4

v5 whole, which is shorter than its diff:
```python
import jax
import jax.numpy as jnp
from jax import lax
from jax.experimental import pallas as pl
from jax.experimental.pallas import tpu as pltpu
from jax.sharding import PartitionSpec as P

MESH = pl.DeviceIdType.MESH
F32 = jnp.float32
BF16 = jnp.bfloat16

D = 2048
EPS = 1e-06
GATE_POWER = 8.0
TOK = 768
BLK = 96
HALF = 384
CH = 128
HID = 704
REACH = 6


def neg_expm1(u):
    series = 1.0 + u * (1.0 / 9.0)
    for n in (8.0, 7.0, 6.0, 5.0, 4.0, 3.0, 2.0):
        series = 1.0 + u * (1.0 / n) * series
    return jnp.where(u > -0.5, -u * series, 1.0 - jnp.exp(u))


def softplus(v):
    tail = jnp.exp(-jnp.abs(v))
    w = tail / (2.0 + tail)
    square = w * w
    series = jnp.full_like(w, 1.0 / 15.0)
    for n in (13.0, 11.0, 9.0, 7.0, 5.0, 3.0, 1.0):
        series = 1.0 / n + square * series
    return jnp.maximum(v, 0.0) + 2.0 * w * series


class TorusGather:
    def __init__(self, buf, rows, here, ring_send, ring_recv, pair_send, pair_recv):
        self.buf, self.rows = buf, rows
        self.z, self.y, self.c, self.t = here
        self.ring_send, self.ring_recv = ring_send, ring_recv
        self.pair_send, self.pair_recv = pair_send, pair_recv
        self.odd = lax.rem(self.y, 2)
        self.mate, self.other = 1 + 2 * self.odd, 3 - 2 * self.odd

    def slot(self, dz, dy):
        return lax.rem(self.z + dz, 4) * 4 + lax.rem(self.y + dy, 4)

    def at(self, half, a, b):
        return (a, b) if half == 0 else (b, a)

    def span(self, half, part):
        quarter = self.rows // 4
        first = half * 2 * quarter
        return (first, 2 * quarter) if part is None else (first + part * quarter, quarter)

    def piece(self, half, where, part=None):
        first, count = self.span(half, part)
        return self.buf.at[self.c, self.slot(*where), pl.ds(first, count)]

    def send(self, half, where, to, part=None):
        ref = self.piece(half, where, part)
        landed = [lax.rem(at + (4 - step), 4) for at, step in zip(where, to)]
        pltpu.make_async_remote_copy(
            src_ref=ref,
            dst_ref=ref,
            send_sem=self.ring_send,
            recv_sem=self.ring_recv.at[half, landed[0] * 4 + landed[1]],
            device_id=(self.slot(*to), self.t),
            device_id_type=MESH,
        ).start()

    def wait(self, half, where):
        ref = self.piece(half, where)
        pltpu.make_async_copy(ref, ref, self.ring_recv.at[half, where[0] * 4 + where[1]]).wait()
        self.pass_over(ref, where)

    def pass_over(self, ref, where):
        dy = where[1]
        if isinstance(dy, int):
            late = {0: 0, 1: self.odd, 2: 1, 3: 1 - self.odd}[dy]
        else:
            late = 0 if dy is self.mate else 1
        pltpu.make_async_remote_copy(
            src_ref=ref,
            dst_ref=ref,
            send_sem=self.pair_send,
            recv_sem=self.pair_recv.at[late],
            device_id=(self.slot(0, 0), self.t + 1 - 2 * self.c),
            device_id_type=MESH,
        ).start()

    def start(self):
        for half in (0, 1):
            for step in (1, 3):
                self.send(half, (0, 0), self.at(half, 0, step))

    def start_second(self):
        for half in (0, 1):
            for step in (1, 3):
                self.send(half, (0, 0), self.at(half, step, 0))
        self.pass_over(self.buf.at[self.c, self.slot(0, 0)], (0, 0))

    def spread(self, half, b, steps=(1, 3)):
        for step in steps:
            self.send(half, self.at(half, 0, b), self.at(half, step, 0))

    def relay(self, half, a, b):
        self.wait(half, self.at(half, a, b))
        self.send(half, self.at(half, a, b), self.at(half, 4 - a, 0))

    def event(self, number):
        at, wait = self.at, self.wait
        mate, other = self.mate, self.other
        if number == 1:
            for half in (0, 1):
                wait(half, at(half, 0, 3))
                self.send(half, at(half, 0, 3), at(half, 0, 1), part=0)
                wait(half, at(half, 0, 1))
                self.send(half, at(half, 0, 1), at(half, 0, 3), part=1)
            self.spread(0, mate)
            self.spread(0, other, (3,))
            self.spread(1, 3)
            self.spread(1, 1)
        if number == 2:
            self.relay(0, 3, 0)
            wait(0, at(0, 1, 0))
            wait(1, at(1, 0, 2))
            self.spread(1, 2)
            wait(0, at(0, 0, 2))
            self.spread(0, 2, (1,))
            self.spread(0, other, (1,))
            self.relay(1, 3, 0)
            wait(1, at(1, 1, 0))
        if number == 3:
            self.relay(0, 1, mate)
            wait(0, at(0, 3, mate))
            self.relay(1, 1, 3)
            wait(1, at(1, 3, 3))
        if number == 4:
            self.relay(0, 1, other)
            self.spread(0, 2, (3,))
            self.relay(1, 3, 1)
            wait(1, at(1, 1, 1))
            wait(0, at(0, 2, 0))
        if number == 5:
            self.relay(0, 3, 2)
            self.relay(1, 1, 2)
            wait(1, at(1, 3, 2))
            wait(0, at(0, 2, mate))
        if number == 6:
            wait(0, at(0, 3, other))
            wait(0, at(0, 2, other))
            wait(1, at(1, 2, 0))
            wait(1, at(1, 2, 3))
        if number == 7:
            wait(0, at(0, 1, 2))
            wait(0, at(0, 2, 2))
            wait(1, at(1, 2, 1))
            wait(1, at(1, 2, 2))

    def wait_pair(self, late):
        ref = self.buf.at[1 - self.c, pl.ds(0, 8)]
        pltpu.make_async_copy(ref, ref, self.pair_recv.at[late]).wait()

    def finish(self):
        ref = self.buf.at[self.c, pl.ds(0, 15)]
        pltpu.make_async_copy(ref, ref, self.ring_send).wait()
        ref = self.buf.at[self.c]
        pltpu.make_async_copy(ref, ref, self.pair_send).wait()


def layer_kernel(
    gate_hbm, rec_hbm, ids_hbm, taps_hbm, gmap_hbm, imap_hbm, level_hbm, extra_hbm, ow_hbm, res_hbm,
    mixg_hbm, preg_hbm, ffng_hbm, gw_hbm, uw_hbm, dw_hbm,
    out_ref,
    gate_ref, rec_ref, ids_ref, taps_ref, gmap_ref, imap_ref, level_ref, extra_ref, res_ref,
    mixg_ref, preg_ref, ffng_ref, gw_ref, uw_ref,
    GU, DW, OW, RP, GP, BH, BA, HX, HI, XF, IDF, FA, DV, S, PR, GL, CS, CB, MX, SQA, SO, XR, ST, SQC, SC, ACC, H,
    PB, RA, RC, PO, FO, FF, PRE, SQB,
    gu_ring, dw_ring, gu_sem, dw_sem, gu_pair, dw_pair, ba_ring, ba_far, ba_sem, ag_ring, ag_far, ra_recv, rc_recv, rs_send, in_sem, sem,
):
    s, t = lax.axis_index("sp"), lax.axis_index("tp")
    z, y = lax.div(s, 4), lax.rem(s, 4)
    x, c = lax.div(t, 2), lax.rem(t, 2)

    def remote(src, dst, send_sem, recv_sem, device):
        copy = pltpu.make_async_remote_copy(
            src_ref=src, dst_ref=dst, send_sem=send_sem, recv_sem=recv_sem, device_id=device, device_id_type=MESH
        )
        copy.start()

    def await_bytes(ref, semaphore):
        pltpu.make_async_copy(ref, ref, semaphore).wait()

    def along_x(step):
        return (s, lax.rem(x + step, 4) * 2 + c)

    partner = (s, t + 1 - 2 * c)
    here = (z, y, c, t)
    gu = TorusGather(GU, 128, here, gu_sem.at[0], gu_ring, gu_sem.at[1], gu_pair)
    dw = TorusGather(DW, HID, here, dw_sem.at[0], dw_ring, dw_sem.at[1], dw_pair)

    barrier = pltpu.get_barrier_semaphore()
    for k in range(1, REACH + 1):
        for peer in (lax.rem(s + k, 16), lax.rem(s + 16 - k, 16)):
            pl.semaphore_signal(barrier, inc=1, device_id=(peer, t), device_id_type=MESH)
    for k in range(1, 8):
        pl.semaphore_signal(barrier, inc=1, device_id=(s, lax.rem(t + k, 8)), device_id_type=MESH)

    own = z * 4 + y
    loads = []
    for src, dst in (
        (gw_hbm, gw_ref), (uw_hbm, uw_ref), (rec_hbm, rec_ref), (ids_hbm, ids_ref), (gate_hbm, gate_ref),
        (taps_hbm, taps_ref), (gmap_hbm, gmap_ref), (imap_hbm, imap_ref), (level_hbm, level_ref),
        (extra_hbm, extra_ref), (mixg_hbm, mixg_ref), (preg_hbm, preg_ref), (ffng_hbm, ffng_ref), (ow_hbm, OW.at[c]),
        (res_hbm, res_ref), (dw_hbm, DW.at[c, own]),
    ):
        loads.append(pltpu.make_async_copy(src, dst, in_sem.at[len(loads)]))
        loads[-1].start()

    loads[0].wait()
    loads[1].wait()
    for i in range(5):
        for n, ref in enumerate((gw_ref, uw_ref)):
            block = ref[128 * i : 128 * i + 128].astype(F32).T.astype(BF16)
            GU[c, own, :, 256 * i + 128 * n : 256 * i + 128 * n + 128] = block
    block = jnp.concatenate([gw_ref[640:704].astype(F32), uw_ref[640:704].astype(F32)], axis=0)
    GU[c, own, :, 1280:1408] = block.T.astype(BF16)
    for load in loads[2:4]:
        load.wait()
    IDF[8:] = jnp.concatenate(
        [jnp.broadcast_to(ids_ref[r : r + 1, :].astype(F32), (128, 128)).T for r in range(6)], axis=0
    )
    XF[8:] = rec_ref[...].astype(F32)

    pl.semaphore_wait(barrier, 2 * REACH + 7)

    after = (lax.rem(s + 1, 16), t)
    remote(rec_ref.at[pl.ds(TOK - 16, 16)], HX, sem.at[0], sem.at[1], after)
    remote(ids_ref, HI, sem.at[2], sem.at[3], after)
    gu.start()
    for load in loads[4:]:
        load.wait()

    RP[c] = res_ref[c]
    GP[c, 0:1] = mixg_ref[...]
    GP[c, 1:2] = preg_ref[...]
    remote(OW.at[c], OW.at[c], ba_sem.at[1], ba_sem.at[2], partner)
    remote(res_ref.at[1 - c], RP.at[c], ba_sem.at[3], ba_sem.at[4], partner)
    remote(GP.at[c], GP.at[c], ba_sem.at[5], ba_sem.at[6], partner)

    for r in range(6):
        rows = slice(128 * r, 128 * r + 128)
        GL[rows] = jax.nn.gelu(gate_ref[rows].astype(F32), approximate=True)
    pair = [
        jnp.concatenate(
            [
                jnp.concatenate([m[0].astype(F32), jnp.zeros((64, 64), F32)], axis=1),
                jnp.concatenate([jnp.zeros((64, 64), F32), m[1].astype(F32)], axis=1),
            ],
            axis=0,
        )
        for m in (gmap_ref, imap_ref)
    ]
    maps = jnp.concatenate(pair, axis=1).astype(BF16)
    rate = -GATE_POWER * softplus(-level_ref[...])
    taps = taps_ref[...].astype(F32)

    def drive(r):
        at = 8 + 128 * r
        ids = IDF[at : at + 128]
        conv = XF[at : at + 128] * taps[0:1]
        for k in (1, 2, 3):
            same = IDF[at - k : at - k + 128] == ids
            conv = conv + jnp.where(same, XF[at - k : at - k + 128], 0.0) * taps[k : k + 1]
        conv = conv.astype(BF16)
        gates = jax.nn.sigmoid(jnp.dot(conv, maps, preferred_element_type=F32))
        rows = slice(128 * r, 128 * r + 128)
        log_decay = rate * gates[:, :CH] + extra_ref[rows]
        FA[rows] = jnp.where(IDF[at - 1 : at + 127] == ids, jnp.exp(log_decay), 0.0)
        DV[rows] = jnp.sqrt(neg_expm1(2.0 * log_decay)) * gates[:, CH:] * conv.astype(F32)

    for r in range(1, 6):
        drive(r)
    await_bytes(HX, sem.at[1])
    await_bytes(HI, sem.at[3])
    XF[0:8] = HX[...].astype(F32)[8:16]
    rim_ids = jnp.broadcast_to(HI[5:6, :].astype(F32), (128, 128)).T[120:128]
    IDF[0:8] = jnp.where(s > 0, rim_ids, -1.0)

    drive(0)

    state = jnp.zeros((8, CH), F32)
    prod = jnp.ones((8, CH), F32)
    for i in range(BLK):
        at = pl.ds(i, 8, stride=BLK)
        f = FA[at, :]
        state = f * state + DV[at, :]
        prod = f * prod
        S[at, :] = state
        PR[at, :] = prod
    befores = []
    p_all, e_all = jnp.ones((1, CH), F32), jnp.zeros((1, CH), F32)
    for b in range(8):
        befores.append((p_all, e_all))
        e_all = prod[b : b + 1] * e_all + state[b : b + 1]
        p_all = prod[b : b + 1] * p_all
    CS[...] = jnp.concatenate([p_all, e_all, jnp.zeros((6, CH), F32)], axis=0)
    for k in range(1, REACH + 1):
        remote(CS, CB.at[k - 1], sem.at[17], sem.at[9], (lax.rem(s + k, 16), t))
    gu.start_second()
    gu.event(1)

    await_bytes(CB, sem.at[9])
    entering = jnp.zeros((1, CH), F32)
    for k in range(REACH, 0, -1):
        entering = jnp.where(s >= k, CB[k - 1, 0:1] * entering + CB[k - 1, 1:2], 0.0)
    for b in range(8):
        rows = slice(BLK * b, BLK * b + BLK)
        p_before, e_before = befores[b]
        states = S[rows] + PR[rows] * (e_before + p_before * entering)
        half, first = b // 4, BLK * (b % 4)
        BH[half, first : first + BLK] = (states * GL[rows]).astype(BF16)

    QUARTER = HALF // 2
    top, bottom = pl.ds(0, QUARTER), pl.ds(QUARTER, QUARTER)
    left, right, across = lax.rem(x + 3, 4), lax.rem(x + 1, 4), lax.rem(x + 2, 4)
    for part, step in ((0, 1), (1, 3), (1, 1), (0, 3)):
        rows = bottom if part else top
        for k in (0, 1):
            remote(
                BH.at[k, rows], BA.at[x, c, rows], ba_sem.at[0], ba_ring.at[0 if step == 1 else 1, c, part],
                (s, lax.rem(x + step, 4) * 2 + k),
            )
    remote(BH.at[1 - c], BA.at[x, c], sem.at[4], sem.at[5], partner)
    BA[x, c] = BH[c]
    for part, step, chip in ((0, 1, left), (1, 3, right)):
        rows = bottom if part else top
        for k in (0, 1):
            await_bytes(BA.at[chip, k, rows], ba_ring.at[0 if step == 1 else 1, k, part])
        ref = BA.at[chip, :, rows]
        remote(ref, ref, ba_sem.at[0], ba_far.at[part], along_x(step))
    gu.event(2)
    for part, step, chip in ((1, 1, left), (0, 3, right)):
        rows = bottom if part else top
        for k in (0, 1):
            await_bytes(BA.at[chip, k, rows], ba_ring.at[0 if step == 1 else 1, k, part])
    await_bytes(BA.at[x, 1 - c], sem.at[5])
    await_bytes(OW.at[1 - c], ba_sem.at[2])
    await_bytes(RP.at[1 - c], ba_sem.at[4])
    await_bytes(GP.at[1 - c], ba_sem.at[6])
    gu.event(3)
    for part in (0, 1):
        await_bytes(BA.at[across, :, bottom if part else top], ba_far.at[part])

    def as_row(square):
        return jnp.broadcast_to(square, (HALF, 128)).T[0:1]

    def chip_sums(ref, send_sem, recv_sem):
        for step in (1, 2, 3):
            remote(ref.at[x], ref.at[x], send_sem, recv_sem, along_x(step))

    def row_factors(ref, count):
        total = ref[0]
        for j in range(1, count):
            total = total + ref[j]
        return jnp.broadcast_to(lax.rsqrt(total * (1.0 / D) + EPS), (128, total.shape[1])).T

    branch = jnp.concatenate([BA[j // 2, j % 2] for j in range(8)], axis=1)
    square = jnp.zeros((HALF, 1), F32)
    for h in (0, 1):
        mixed = jnp.dot(branch, OW[h], preferred_element_type=F32).astype(BF16).astype(F32)
        MX[h] = mixed
        square = square + jnp.sum(mixed * mixed, axis=1, keepdims=True)
    SQA[x] = as_row(square)
    chip_sums(SQA, sem.at[10], sem.at[11])
    dw.start()
    gu.event(4)
    await_bytes(SQA.at[pl.ds(0, 3)], sem.at[11])
    factor = row_factors(SQA, 4)
    factor = jnp.concatenate([factor, factor], axis=1)
    square = jnp.zeros((HALF, 1), F32)
    for h in (0, 1):
        stream = (RP[h].astype(F32) + MX[h] * factor * GP[h, 0:1]).astype(BF16)
        SO[h] = stream
        stream = stream.astype(F32)
        ST[x, h] = (stream * GP[h, 1:2]).astype(BF16)
        square = square + jnp.sum(stream * stream, axis=1, keepdims=True)
    SQC[x] = as_row(square)
    chip_sums(SQC, sem.at[6], sem.at[7])

    for part, step in ((0, 1), (1, 3), (1, 1), (0, 3)):
        ref = ST.at[x, :, bottom if part else top]
        remote(ref, ref, sem.at[12], ag_ring.at[0 if step == 1 else 1, part], along_x(step))
    remote(SO.at[1 - c], XR, sem.at[15], sem.at[16], partner)
    gu.event(5)
    dw.start_second()

    early = lax.div(y, 2)

    def product(q, h, tile):
        rows = pl.ds(4 * q + 2 * h, 2)
        if tile < 10:
            p, i = tile // 5, tile % 5
            weights = GU[p, rows, :, 256 * i : 256 * i + 256].reshape(256, 256)
        else:
            weights = jnp.concatenate([GU[p, rows, :, 1280:1408].reshape(256, 128) for p in (0, 1)], axis=1)
        return jnp.dot(ST[q, h], weights, preferred_element_type=F32)

    def gather_in(tiles):
        for tile in tiles:
            total = ACC[tile]
            for q in (x, left, right):
                total = total + product(q, 1 - early, tile)
            ACC[tile] = total

    def hidden(tiles):
        factor = SC[...]
        for tile in tiles:
            both = ACC[tile] + product(across, early, tile) + product(across, 1 - early, tile)
            if tile < 10:
                p, i = tile // 5, tile % 5
                act = jax.nn.silu(both[:, :128] * factor) * (both[:, 128:] * factor)
                H[p, :, 128 * i : 128 * i + 128] = act.astype(BF16)
            else:
                for p in (0, 1):
                    tail = both[:, 128 * p : 128 * p + 128] * factor
                    H[p, :, 640:704] = (jax.nn.silu(tail[:, :64]) * tail[:, 64:]).astype(BF16)

    dw.event(1)
    for part, step, chip in ((0, 1, left), (1, 3, right)):
        ref = ST.at[chip, :, bottom if part else top]
        await_bytes(ref, ag_ring.at[0 if step == 1 else 1, part])
        remote(ref, ref, sem.at[12], ag_far.at[part], along_x(step))
    gu.event(6)
    gu.wait_pair(0)
    for tile in range(11):
        ACC[tile] = product(x, early, tile)
    gu.event(7)
    for part, step, chip in ((1, 1, left), (0, 3, right)):
        await_bytes(ST.at[chip, :, bottom if part else top], ag_ring.at[0 if step == 1 else 1, part])
    for tile in range(11):
        ACC[tile] = ACC[tile] + product(left, early, tile) + product(right, early, tile)
    dw.event(2)
    gu.wait_pair(1)
    gather_in(range(6))
    dw.event(3)
    gather_in(range(6, 11))
    await_bytes(SQC.at[pl.ds(0, 3)], sem.at[7])
    SC[...] = row_factors(SQC, 4)
    for part in (0, 1):
        await_bytes(ST.at[across, :, bottom if part else top], ag_far.at[part])
    hidden(range(6))
    dw.event(4)
    hidden(range(6, 11))
    dw.event(5)

    def down_of(p, chip, h):
        weights = jnp.concatenate([DW[p, 4 * chip + 2 * h], DW[p, 4 * chip + 2 * h + 1]], axis=1)
        return jnp.dot(H[p], weights, preferred_element_type=F32)

    def down(chip, h):
        return down_of(c, chip, h) + down_of(1 - c, chip, h)

    def scatter_across(n, h):
        PB[n, 0] = (PRE[0] + down_of(1 - c, across, h)).astype(BF16)
        for m, (rows, step) in enumerate(((top, 1), (bottom, 3))):
            remote(PB.at[n, 0, rows], RA.at[n, m], rs_send.at[n, m], ra_recv.at[n, m], along_x(step))

    def own_products(h):
        for m, chip in enumerate((across, right, left)):
            PRE[m] = down_of(c, chip, h)

    def scatter_near(n, h):
        for m, (chip, rows) in enumerate(((right, bottom), (left, top))):
            total = PRE[1 + m] + down_of(1 - c, chip, h)
            PB[n, 1 + m] = total.astype(BF16)
            FO[n, m] = total[:QUARTER] if m == 0 else total[QUARTER:]
            remote(
                PB.at[n, 1 + m, rows], RC.at[m, c, rows], rs_send.at[n, 2 + m], rc_recv.at[m, c, 1 - m],
                (s, 2 * chip + h),
            )

    def scatter_relay(n, h):
        for m, (chip, rows) in enumerate(((right, top), (left, bottom))):
            await_bytes(RA.at[n, m], ra_recv.at[n, m])
            PB[n, 1 + m, rows] = (FO[n, m] + RA[n, m].astype(F32)).astype(BF16)
            remote(
                PB.at[n, 1 + m, rows], RC.at[m, c, rows], rs_send.at[n, 4 + m], rc_recv.at[m, c, m],
                (s, 2 * chip + h),
            )

    own_products(early)
    dw.wait_pair(0)
    scatter_across(0, early)
    dw.event(6)
    scatter_near(0, early)
    dw.event(7)
    own_products(1 - early)
    dw.wait_pair(1)
    scatter_across(1, 1 - early)
    scatter_relay(0, early)
    scatter_near(1, 1 - early)
    PB[0, 3] = down(x, 1 - c).astype(BF16)
    remote(PB.at[0, 3], PO.at[c], sem.at[8], sem.at[18], partner)
    scatter_relay(1, 1 - early)
    PO[c] = down(x, c).astype(BF16)
    await_bytes(PO.at[1 - c], sem.at[18])
    sums = []
    for k in (0, 1):
        for m in (0, 1):
            for part, rows in ((0, top), (1, bottom)):
                await_bytes(RC.at[m, k, rows], rc_recv.at[m, k, part])
        total = PO[k].astype(F32) + RC[0, k].astype(F32) + RC[1, k].astype(F32)
        total = total.astype(BF16).astype(F32)
        FF[k] = total
        square = jnp.sum(total * total, axis=1, keepdims=True)
        sums.append(as_row(square))

    SQB[t] = jnp.concatenate(sums, axis=1)
    for k in range(1, 8):
        remote(SQB.at[t], SQB.at[t], sem.at[13], sem.at[14], (s, lax.rem(t + k, 8)))
    await_bytes(XR, sem.at[16])
    await_bytes(SQB.at[pl.ds(0, 7)], sem.at[14])
    factors = row_factors(SQB, 8)
    for k in (0, 1):
        factor = factors[HALF * k : HALF * k + HALF]
        FF[k] = FF[k] * jnp.concatenate([factor, factor], axis=1) * ffng_ref[...]
    out_ref[c] = (SO[c].astype(F32) + FF[c]).astype(BF16)
    out_ref[1 - c] = (XR[...].astype(F32) + FF[1 - c]).astype(BF16)

    gu.finish()
    dw.finish()
    await_bytes(HX, sem.at[0])
    await_bytes(HI, sem.at[2])
    await_bytes(CB, sem.at[17])
    await_bytes(BA.at[pl.ds(0, 3)], ba_sem.at[0])
    await_bytes(OW.at[c], ba_sem.at[1])
    await_bytes(RP.at[c], ba_sem.at[3])
    await_bytes(GP.at[c], ba_sem.at[5])
    await_bytes(BH.at[0], sem.at[4])
    await_bytes(SQA.at[pl.ds(0, 3)], sem.at[10])
    await_bytes(SQC.at[pl.ds(0, 3)], sem.at[6])
    await_bytes(XR, sem.at[15])
    await_bytes(ST.at[pl.ds(0, 3)], sem.at[12])
    for n in (0, 1):
        for m in range(6):
            await_bytes(PB.at[0, 0, top], rs_send.at[n, m])
    await_bytes(PB.at[0, 3], sem.at[8])
    await_bytes(SQB.at[pl.ds(0, 7)], sem.at[13])


def body(
    gate_branch, recur_input, doc_ids, conv_taps, gate_map, input_map, decay_level, decay_extra, out_weight,
    residual, mix_gain, pre_gain, ffn_gain, gate_weight, up_weight, down_weight,
):
    vmem = pl.BlockSpec(memory_space=pltpu.VMEM)
    dma = pltpu.SemaphoreType.DMA
    out = pl.pallas_call(
        layer_kernel,
        name="layer",
        out_shape=pltpu.VMEM((2, HALF, 256), BF16),
        in_specs=[pl.BlockSpec(memory_space=pl.ANY)] * 16,
        out_specs=vmem,
        scratch_shapes=[
            pltpu.VMEM((TOK, CH), BF16),
            pltpu.VMEM((TOK, CH), BF16),
            pltpu.VMEM((6, 128), jnp.int32),
            pltpu.VMEM((4, CH), BF16),
            pltpu.VMEM((2, 64, 64), BF16),
            pltpu.VMEM((2, 64, 64), BF16),
            pltpu.VMEM((1, CH), F32),
            pltpu.VMEM((TOK, CH), F32),
            pltpu.VMEM((2, HALF, 256), BF16),
            pltpu.VMEM((1, 256), F32),
            pltpu.VMEM((1, 256), F32),
            pltpu.VMEM((1, 256), F32),
            pltpu.VMEM((HID, 128), BF16),
            pltpu.VMEM((HID, 128), BF16),
            pltpu.VMEM((2, 16, 128, 1408), BF16),
            pltpu.VMEM((2, 16, HID, 128), BF16),
            pltpu.VMEM((2, 1024, 256), BF16),
            pltpu.VMEM((2, HALF, 256), BF16),
            pltpu.VMEM((2, 8, 256), F32),
            pltpu.VMEM((2, HALF, CH), BF16),
            pltpu.VMEM((4, 2, HALF, CH), BF16),
            pltpu.VMEM((16, CH), BF16),
            pltpu.VMEM((6, 128), jnp.int32),
            pltpu.VMEM((TOK + 8, CH), F32),
            pltpu.VMEM((TOK + 8, CH), F32),
            pltpu.VMEM((TOK, CH), F32),
            pltpu.VMEM((TOK, CH), F32),
            pltpu.VMEM((TOK, CH), F32),
            pltpu.VMEM((TOK, CH), F32),
            pltpu.VMEM((TOK, CH), F32),
            pltpu.VMEM((8, CH), F32),
            pltpu.VMEM((REACH, 8, CH), F32),
            pltpu.VMEM((2, HALF, 256), F32),
            pltpu.VMEM((4, 1, HALF), F32),
            pltpu.VMEM((2, HALF, 256), BF16),
            pltpu.VMEM((HALF, 256), BF16),
            pltpu.VMEM((4, 2, HALF, 256), BF16),
            pltpu.VMEM((4, 1, HALF), F32),
            pltpu.VMEM((HALF, 128), F32),
            pltpu.VMEM((11, HALF, 256), F32),
            pltpu.VMEM((2, HALF, HID), BF16),
            pltpu.VMEM((2, 4, HALF, 256), BF16),
            pltpu.VMEM((2, 2, HALF // 2, 256), BF16),
            pltpu.VMEM((2, 2, HALF, 256), BF16),
            pltpu.VMEM((2, HALF, 256), BF16),
            pltpu.VMEM((2, 2, HALF // 2, 256), F32),
            pltpu.VMEM((2, HALF, 256), F32),
            pltpu.VMEM((3, HALF, 256), F32),
            pltpu.VMEM((8, 1, TOK), F32),
            dma((2, 16)),
            dma((2, 16)),
            dma((2,)),
            dma((2,)),
            dma((2,)),
            dma((2,)),
            dma((2, 2, 2)),
            dma((2,)),
            dma((7,)),
            dma((2, 2)),
            dma((2,)),
            dma((2, 2)),
            dma((2, 2, 2)),
            dma((2, 6)),
            dma((16,)),
            dma((19,)),
        ],
        compiler_params=pltpu.CompilerParams(
            collective_id=0, has_side_effects=True, vmem_limit_bytes=60 * 1024 * 1024
        ),
    )(
        gate_branch,
        recur_input,
        doc_ids.reshape(6, 128),
        conv_taps,
        gate_map,
        input_map,
        decay_level.reshape(1, CH),
        decay_extra,
        out_weight,
        residual.reshape(2, HALF, 256),
        mix_gain.reshape(1, 256),
        pre_gain.reshape(1, 256),
        ffn_gain.reshape(1, 256),
        gate_weight.T,
        up_weight.T,
        down_weight,
    )
    return out.reshape(TOK, 256)


def solution(mesh):
    return jax.shard_map(
        body,
        mesh=mesh,
        in_specs=(
            P("sp", "tp"),
            P("sp", "tp"),
            P("sp"),
            P(None, "tp"),
            P("tp", None, None),
            P("tp", None, None),
            P("tp"),
            P("sp", "tp"),
            P(None, "tp"),
            P("sp", "tp"),
            P("tp"),
            P("tp"),
            P("tp"),
            P("sp", "tp"),
            P("sp", "tp"),
            P("tp", "sp"),
        ),
        out_specs=P("sp", "tp"),
        check_vma=False,
    )
```

time: 76.7 us -> 74.6 us (0.973)
  Pallas kernels: 75.8 us -> 73.7 us
    pallas_call x1, Pallas kernels: 75.8 us -> 73.7 us  [body(): pl.pallas_call(layer_kernel, name='layer', out_shape=pltpu.VMEM((2, HALF,...]
where the time goes in v5:
time: 74.6 us; the launch traced here: 74.4 us
  Pallas kernels  73.7 us (99%)
  local copies, waits for them, and re-layouts  0.75 us (1%)
    pallas_call x1, Pallas kernels, body(): pl.pallas_call(layer_kernel, name='layer', out_shape=pltpu.VMEM((2, HALF,...  73.7 us

profile of v5, /device:TPU:1, one launch (start us, length us, event | category | flops | bytes accessed | tf_op | source)
XLA Modules:
  0.0 74.4 jit_solution(16007557474537762482)
XLA Ops:
  0.0 73.7 %layer.1 = bf16[2,384,256]{2,1,0:T(8,128)(2,1)S(1)} custom-call(bf16[768,128]{1,0:T(8,128)(2,1)} %gate_hbm.1, bf16[768,128]{1,0:T(8,128)(2,1)} %rec_hbm.1, s32[6,128]{1,0:T(8,128)} %bitcast.13, bf16[4,128]{1,0:T(4,128)(2,1)} %taps_hbm.1, bf16[2,64,64]{2,1,0:T(8,128)(2,1)} %gmap_hbm.1, bf16[2,64,64]{2,1,0:T(8,128)(2,1)} %imap_hbm.1, f32[1,128]{1,0:T(1,128)} %bitcast.17, ...), custom_call_target="tpu_custom_call" | custom-call | tf_op jit(solution)/shard_map/layer/pallas_call | solution.py:563
  73.7 0.7 %copy.18 = bf16[768,256]{1,0:T(8,128)(2,1)} copy(bf16[768,256]{1,0:T(8,128)(2,1)S(1)} %bitcast.9) | data formatting | bytes 786432

commit v6 on v5

--- a/solution.py
+++ b/solution.py
@@ -37,6 +37,23 @@
     return jnp.maximum(v, 0.0) + 2.0 * w * series
 
 
+TOGETHER = (
+    ((0, 0, 3), (0, 0, 1)),
+    ((1, 3, 0), (1, 1, 0)),
+    ((0, 1, 0), (1, 0, 1)),
+    ((0, 3, "m"), (1, 3, 3)),
+    ((1, 1, 1), (0, 2, 0)),
+    ((1, 2, 3), (0, 2, "m")),
+    ((0, 3, "o"), (0, 2, "o"), (1, 0, 2), (1, 3, 2)),
+    ((0, 1, 2), (0, 2, 2), (1, 1, 2), (1, 2, 2)),
+)
+ALONE = (
+    (0, 0, 2), (1, 2, 0), (0, 3, 0), (0, 1, "m"), (0, 1, "o"), (0, 3, 2),
+    (1, 0, 3), (1, 3, 1), (1, 1, 3), (1, 2, 1),
+)
+GROUPS = (*TOGETHER, *((one,) for one in ALONE))
+
+
 class TorusGather:
     def __init__(self, buf, rows, here, ring_send, ring_recv, pair_send, pair_recv):
         self.buf, self.rows = buf, rows
@@ -61,22 +78,37 @@
         first, count = self.span(half, part)
         return self.buf.at[self.c, self.slot(*where), pl.ds(first, count)]
 
+    def named(self, dy):
+        return dy if isinstance(dy, int) else "m" if dy is self.mate else "o"
+
+    def group(self, half, where):
+        key = (half, where[0], self.named(where[1]))
+        return next(n for n, keys in enumerate(GROUPS) if key in keys)
+
     def send(self, half, where, to, part=None):
         ref = self.piece(half, where, part)
-        landed = [lax.rem(at + (4 - step), 4) for at, step in zip(where, to)]
+        dz, dy = (where[0] - to[0]) % 4, where[1]
+        if isinstance(dy, int):
+            dy = (dy - to[1]) % 4
         pltpu.make_async_remote_copy(
             src_ref=ref,
             dst_ref=ref,
             send_sem=self.ring_send,
-            recv_sem=self.ring_recv.at[half, landed[0] * 4 + landed[1]],
+            recv_sem=self.ring_recv.at[self.group(half, (dz, dy))],
             device_id=(self.slot(*to), self.t),
             device_id_type=MESH,
         ).start()
 
-    def wait(self, half, where):
-        ref = self.piece(half, where)
-        pltpu.make_async_copy(ref, ref, self.ring_recv.at[half, where[0] * 4 + where[1]]).wait()
-        self.pass_over(ref, where)
+    def wait(self, *pieces):
+        number = self.group(*pieces[0])
+        assert len(pieces) == len(GROUPS[number])
+        assert all(self.group(*piece) == number for piece in pieces)
+        ref = self.piece(*pieces[0])
+        if len(pieces) > 1:
+            ref = self.buf.at[self.c, pl.ds(0, len(pieces) // 2)]
+        pltpu.make_async_copy(ref, ref, self.ring_recv.at[number]).wait()
+        for half, where in pieces:
+            self.pass_over(self.piece(half, where), where)
 
     def pass_over(self, ref, where):
         dy = where[1]
@@ -109,7 +141,7 @@
             self.send(half, self.at(half, 0, b), self.at(half, step, 0))
 
     def relay(self, half, a, b):
-        self.wait(half, self.at(half, a, b))
+        self.wait((half, self.at(half, a, b)))
         self.send(half, self.at(half, a, b), self.at(half, 4 - a, 0))
 
     def event(self, number):
@@ -117,9 +149,8 @@
         mate, other = self.mate, self.other
         if number == 1:
             for half in (0, 1):
-                wait(half, at(half, 0, 3))
+                wait((half, at(half, 0, 3)), (half, at(half, 0, 1)))
                 self.send(half, at(half, 0, 3), at(half, 0, 1), part=0)
-                wait(half, at(half, 0, 1))
                 self.send(half, at(half, 0, 1), at(half, 0, 3), part=1)
             self.spread(0, mate)
             self.spread(0, other, (3,))
@@ -127,40 +158,30 @@
             self.spread(1, 1)
         if number == 2:
             self.relay(0, 3, 0)
-            wait(0, at(0, 1, 0))
-            wait(1, at(1, 0, 2))
+            wait((1, at(1, 0, 2)))
             self.spread(1, 2)
-            wait(0, at(0, 0, 2))
+            wait((0, at(0, 0, 2)))
             self.spread(0, 2, (1,))
             self.spread(0, other, (1,))
             self.relay(1, 3, 0)
-            wait(1, at(1, 1, 0))
+            wait((0, at(0, 1, 0)), (1, at(1, 1, 0)))
         if number == 3:
             self.relay(0, 1, mate)
-            wait(0, at(0, 3, mate))
             self.relay(1, 1, 3)
-            wait(1, at(1, 3, 3))
+            wait((0, at(0, 3, mate)), (1, at(1, 3, 3)))
         if number == 4:
             self.relay(0, 1, other)
             self.spread(0, 2, (3,))
             self.relay(1, 3, 1)
-            wait(1, at(1, 1, 1))
-            wait(0, at(0, 2, 0))
+            wait((1, at(1, 1, 1)), (0, at(0, 2, 0)))
         if number == 5:
+            self.relay(1, 1, 2)
+            wait((1, at(1, 3, 2)), (0, at(0, 2, mate)))
             self.relay(0, 3, 2)
-            self.relay(1, 1, 2)
-            wait(1, at(1, 3, 2))
-            wait(0, at(0, 2, mate))
         if number == 6:
-            wait(0, at(0, 3, other))
-            wait(0, at(0, 2, other))
-            wait(1, at(1, 2, 0))
-            wait(1, at(1, 2, 3))
+            wait((0, at(0, 3, other)), (0, at(0, 2, other)), (1, at(1, 2, 0)), (1, at(1, 2, 3)))
         if number == 7:
-            wait(0, at(0, 1, 2))
-            wait(0, at(0, 2, 2))
-            wait(1, at(1, 2, 1))
-            wait(1, at(1, 2, 2))
+            wait((0, at(0, 1, 2)), (0, at(0, 2, 2)), (1, at(1, 2, 1)), (1, at(1, 2, 2)))
 
     def wait_pair(self, late):
         ref = self.buf.at[1 - self.c, pl.ds(0, 8)]
@@ -181,7 +202,7 @@
     mixg_ref, preg_ref, ffng_ref, gw_ref, uw_ref,
     GU, DW, OW, RP, GP, BH, BA, HX, HI, XF, IDF, FA, DV, S, PR, GL, CS, CB, MX, SQA, SO, XR, ST, SQC, SC, ACC, H,
     PB, RA, RC, PO, FO, FF, PRE, SQB,
-    gu_ring, dw_ring, gu_sem, dw_sem, gu_pair, dw_pair, ba_ring, ba_far, ba_sem, ag_ring, ag_far, ra_recv, rc_recv, rs_send, in_sem, sem,
+    gu_ring, dw_ring, gu_pair, dw_pair, ba_ring, ag_ring, ra_recv, rc_recv, own_sem, sem,
 ):
     s, t = lax.axis_index("sp"), lax.axis_index("tp")
     z, y = lax.div(s, 4), lax.rem(s, 4)
@@ -201,8 +222,8 @@
 
     partner = (s, t + 1 - 2 * c)
     here = (z, y, c, t)
-    gu = TorusGather(GU, 128, here, gu_sem.at[0], gu_ring, gu_sem.at[1], gu_pair)
-    dw = TorusGather(DW, HID, here, dw_sem.at[0], dw_ring, dw_sem.at[1], dw_pair)
+    gu = TorusGather(GU, 128, here, own_sem.at[2], gu_ring, own_sem.at[3], gu_pair)
+    dw = TorusGather(DW, HID, here, own_sem.at[14], dw_ring, own_sem.at[15], dw_pair)
 
     barrier = pltpu.get_barrier_semaphore()
     for k in range(1, REACH + 1):
@@ -219,7 +240,7 @@
         (extra_hbm, extra_ref), (mixg_hbm, mixg_ref), (preg_hbm, preg_ref), (ffng_hbm, ffng_ref), (ow_hbm, OW.at[c]),
         (res_hbm, res_ref), (dw_hbm, DW.at[c, own]),
     ):
-        loads.append(pltpu.make_async_copy(src, dst, in_sem.at[len(loads)]))
+        loads.append(pltpu.make_async_copy(src, dst, own_sem.at[len(loads)]))
         loads[-1].start()
 
     loads[0].wait()
@@ -240,8 +261,8 @@
     pl.semaphore_wait(barrier, 2 * REACH + 7)
 
     after = (lax.rem(s + 1, 16), t)
-    remote(rec_ref.at[pl.ds(TOK - 16, 16)], HX, sem.at[0], sem.at[1], after)
-    remote(ids_ref, HI, sem.at[2], sem.at[3], after)
+    remote(rec_ref.at[pl.ds(TOK - 16, 16)], HX, own_sem.at[0], sem.at[0], after)
+    remote(ids_ref, HI, own_sem.at[1], sem.at[1], after)
     gu.start()
     for load in loads[4:]:
         load.wait()
@@ -249,9 +270,9 @@
     RP[c] = res_ref[c]
     GP[c, 0:1] = mixg_ref[...]
     GP[c, 1:2] = preg_ref[...]
-    remote(OW.at[c], OW.at[c], ba_sem.at[1], ba_sem.at[2], partner)
-    remote(res_ref.at[1 - c], RP.at[c], ba_sem.at[3], ba_sem.at[4], partner)
-    remote(GP.at[c], GP.at[c], ba_sem.at[5], ba_sem.at[6], partner)
+    remote(OW.at[c], OW.at[c], own_sem.at[4], sem.at[9], partner)
+    remote(res_ref.at[1 - c], RP.at[c], own_sem.at[5], sem.at[10], partner)
+    remote(GP.at[c], GP.at[c], own_sem.at[6], sem.at[11], partner)
 
     for r in range(6):
         rows = slice(128 * r, 128 * r + 128)
@@ -286,8 +307,8 @@
 
     for r in range(1, 6):
         drive(r)
-    await_bytes(HX, sem.at[1])
-    await_bytes(HI, sem.at[3])
+    await_bytes(HX, sem.at[0])
+    await_bytes(HI, sem.at[1])
     XF[0:8] = HX[...].astype(F32)[8:16]
     rim_ids = jnp.broadcast_to(HI[5:6, :].astype(F32), (128, 128)).T[120:128]
     IDF[0:8] = jnp.where(s > 0, rim_ids, -1.0)
@@ -311,11 +332,11 @@
         p_all = prod[b : b + 1] * p_all
     CS[...] = jnp.concatenate([p_all, e_all, jnp.zeros((6, CH), F32)], axis=0)
     for k in range(1, REACH + 1):
-        remote(CS, CB.at[k - 1], sem.at[17], sem.at[9], (lax.rem(s + k, 16), t))
+        remote(CS, CB.at[k - 1], own_sem.at[7], sem.at[2], (lax.rem(s + k, 16), t))
     gu.start_second()
     gu.event(1)
 
-    await_bytes(CB, sem.at[9])
+    await_bytes(CB, sem.at[2])
     entering = jnp.zeros((1, CH), F32)
     for k in range(REACH, 0, -1):
         entering = jnp.where(s >= k, CB[k - 1, 0:1] * entering + CB[k - 1, 1:2], 0.0)
@@ -333,29 +354,26 @@
         rows = bottom if part else top
         for k in (0, 1):
             remote(
-                BH.at[k, rows], BA.at[x, c, rows], ba_sem.at[0], ba_ring.at[0 if step == 1 else 1, c, part],
+                BH.at[k, rows], BA.at[x, c, rows], own_sem.at[8], ba_ring.at[0 if step == 1 else 1, part],
                 (s, lax.rem(x + step, 4) * 2 + k),
             )
-    remote(BH.at[1 - c], BA.at[x, c], sem.at[4], sem.at[5], partner)
+    remote(BH.at[1 - c], BA.at[x, c], own_sem.at[9], sem.at[5], partner)
     BA[x, c] = BH[c]
     for part, step, chip in ((0, 1, left), (1, 3, right)):
         rows = bottom if part else top
-        for k in (0, 1):
-            await_bytes(BA.at[chip, k, rows], ba_ring.at[0 if step == 1 else 1, k, part])
         ref = BA.at[chip, :, rows]
-        remote(ref, ref, ba_sem.at[0], ba_far.at[part], along_x(step))
+        await_bytes(ref, ba_ring.at[0 if step == 1 else 1, part])
+        remote(ref, ref, own_sem.at[8], ba_ring.at[2, 0], along_x(step))
     gu.event(2)
     for part, step, chip in ((1, 1, left), (0, 3, right)):
         rows = bottom if part else top
-        for k in (0, 1):
-            await_bytes(BA.at[chip, k, rows], ba_ring.at[0 if step == 1 else 1, k, part])
+        await_bytes(BA.at[chip, :, rows], ba_ring.at[0 if step == 1 else 1, part])
     await_bytes(BA.at[x, 1 - c], sem.at[5])
-    await_bytes(OW.at[1 - c], ba_sem.at[2])
-    await_bytes(RP.at[1 - c], ba_sem.at[4])
-    await_bytes(GP.at[1 - c], ba_sem.at[6])
+    await_bytes(OW.at[1 - c], sem.at[9])
+    await_bytes(RP.at[1 - c], sem.at[10])
+    await_bytes(GP.at[1 - c], sem.at[11])
     gu.event(3)
-    for part in (0, 1):
-        await_bytes(BA.at[across, :, bottom if part else top], ba_far.at[part])
+    await_bytes(BA.at[across], ba_ring.at[2, 0])
 
     def as_row(square):
         return jnp.broadcast_to(square, (HALF, 128)).T[0:1]
@@ -377,10 +395,10 @@
         MX[h] = mixed
         square = square + jnp.sum(mixed * mixed, axis=1, keepdims=True)
     SQA[x] = as_row(square)
-    chip_sums(SQA, sem.at[10], sem.at[11])
+    chip_sums(SQA, own_sem.at[10], sem.at[3])
     dw.start()
     gu.event(4)
-    await_bytes(SQA.at[pl.ds(0, 3)], sem.at[11])
+    await_bytes(SQA.at[pl.ds(0, 3)], sem.at[3])
     factor = row_factors(SQA, 4)
     factor = jnp.concatenate([factor, factor], axis=1)
     square = jnp.zeros((HALF, 1), F32)
@@ -391,12 +409,12 @@
         ST[x, h] = (stream * GP[h, 1:2]).astype(BF16)
         square = square + jnp.sum(stream * stream, axis=1, keepdims=True)
     SQC[x] = as_row(square)
-    chip_sums(SQC, sem.at[6], sem.at[7])
+    chip_sums(SQC, own_sem.at[11], sem.at[4])
 
     for part, step in ((0, 1), (1, 3), (1, 1), (0, 3)):
         ref = ST.at[x, :, bottom if part else top]
-        remote(ref, ref, sem.at[12], ag_ring.at[0 if step == 1 else 1, part], along_x(step))
-    remote(SO.at[1 - c], XR, sem.at[15], sem.at[16], partner)
+        remote(ref, ref, own_sem.at[12], ag_ring.at[0 if step == 1 else 1, part], along_x(step))
+    remote(SO.at[1 - c], XR, own_sem.at[13], sem.at[6], partner)
     gu.event(5)
     dw.start_second()
 
@@ -435,7 +453,7 @@
     for part, step, chip in ((0, 1, left), (1, 3, right)):
         ref = ST.at[chip, :, bottom if part else top]
         await_bytes(ref, ag_ring.at[0 if step == 1 else 1, part])
-        remote(ref, ref, sem.at[12], ag_far.at[part], along_x(step))
+        remote(ref, ref, own_sem.at[12], ag_ring.at[2, 0], along_x(step))
     gu.event(6)
     gu.wait_pair(0)
     for tile in range(11):
@@ -450,10 +468,9 @@
     gather_in(range(6))
     dw.event(3)
     gather_in(range(6, 11))
-    await_bytes(SQC.at[pl.ds(0, 3)], sem.at[7])
+    await_bytes(SQC.at[pl.ds(0, 3)], sem.at[4])
     SC[...] = row_factors(SQC, 4)
-    for part in (0, 1):
-        await_bytes(ST.at[across, :, bottom if part else top], ag_far.at[part])
+    await_bytes(ST.at[across], ag_ring.at[2, 0])
     hidden(range(6))
     dw.event(4)
     hidden(range(6, 11))
@@ -469,7 +486,7 @@
     def scatter_across(n, h):
         PB[n, 0] = (PRE[0] + down_of(1 - c, across, h)).astype(BF16)
         for m, (rows, step) in enumerate(((top, 1), (bottom, 3))):
-            remote(PB.at[n, 0, rows], RA.at[n, m], rs_send.at[n, m], ra_recv.at[n, m], along_x(step))
+            remote(PB.at[n, 0, rows], RA.at[n, m], own_sem.at[16], ra_recv.at[n, m], along_x(step))
 
     def own_products(h):
         for m, chip in enumerate((across, right, left)):
@@ -481,7 +498,7 @@
             PB[n, 1 + m] = total.astype(BF16)
             FO[n, m] = total[:QUARTER] if m == 0 else total[QUARTER:]
             remote(
-                PB.at[n, 1 + m, rows], RC.at[m, c, rows], rs_send.at[n, 2 + m], rc_recv.at[m, c, 1 - m],
+                PB.at[n, 1 + m, rows], RC.at[m, c, rows], own_sem.at[16], rc_recv.at[0],
                 (s, 2 * chip + h),
             )
 
@@ -490,7 +507,7 @@
             await_bytes(RA.at[n, m], ra_recv.at[n, m])
             PB[n, 1 + m, rows] = (FO[n, m] + RA[n, m].astype(F32)).astype(BF16)
             remote(
-                PB.at[n, 1 + m, rows], RC.at[m, c, rows], rs_send.at[n, 4 + m], rc_recv.at[m, c, m],
+                PB.at[n, 1 + m, rows], RC.at[m, c, rows], own_sem.at[16], rc_recv.at[1],
                 (s, 2 * chip + h),
             )
 
@@ -506,26 +523,28 @@
     scatter_relay(0, early)
     scatter_near(1, 1 - early)
     PB[0, 3] = down(x, 1 - c).astype(BF16)
-    remote(PB.at[0, 3], PO.at[c], sem.at[8], sem.at[18], partner)
+    remote(PB.at[0, 3], PO.at[c], own_sem.at[17], sem.at[8], partner)
     scatter_relay(1, 1 - early)
     PO[c] = down(x, c).astype(BF16)
-    await_bytes(PO.at[1 - c], sem.at[18])
+    await_bytes(PO.at[1 - c], sem.at[8])
+    await_bytes(RC.at[0], rc_recv.at[0])
+    for k in (0, 1):
+        FF[k, :QUARTER] = PO[k, :QUARTER].astype(F32) + RC[1, k, :QUARTER].astype(F32)
+        FF[k, QUARTER:] = PO[k, QUARTER:].astype(F32) + RC[0, k, QUARTER:].astype(F32)
+    await_bytes(RC.at[0], rc_recv.at[1])
     sums = []
     for k in (0, 1):
-        for m in (0, 1):
-            for part, rows in ((0, top), (1, bottom)):
-                await_bytes(RC.at[m, k, rows], rc_recv.at[m, k, part])
-        total = PO[k].astype(F32) + RC[0, k].astype(F32) + RC[1, k].astype(F32)
-        total = total.astype(BF16).astype(F32)
+        last = jnp.concatenate([RC[0, k, :QUARTER], RC[1, k, QUARTER:]], axis=0)
+        total = (FF[k] + last.astype(F32)).astype(BF16).astype(F32)
         FF[k] = total
         square = jnp.sum(total * total, axis=1, keepdims=True)
         sums.append(as_row(square))
 
     SQB[t] = jnp.concatenate(sums, axis=1)
     for k in range(1, 8):
-        remote(SQB.at[t], SQB.at[t], sem.at[13], sem.at[14], (s, lax.rem(t + k, 8)))
-    await_bytes(XR, sem.at[16])
-    await_bytes(SQB.at[pl.ds(0, 7)], sem.at[14])
+        remote(SQB.at[t], SQB.at[t], own_sem.at[18], sem.at[7], (s, lax.rem(t + k, 8)))
+    await_bytes(XR, sem.at[6])
+    await_bytes(SQB.at[pl.ds(0, 7)], sem.at[7])
     factors = row_factors(SQB, 8)
     for k in (0, 1):
         factor = factors[HALF * k : HALF * k + HALF]
@@ -535,23 +554,21 @@
 
     gu.finish()
     dw.finish()
-    await_bytes(HX, sem.at[0])
-    await_bytes(HI, sem.at[2])
-    await_bytes(CB, sem.at[17])
-    await_bytes(BA.at[pl.ds(0, 3)], ba_sem.at[0])
-    await_bytes(OW.at[c], ba_sem.at[1])
-    await_bytes(RP.at[c], ba_sem.at[3])
-    await_bytes(GP.at[c], ba_sem.at[5])
-    await_bytes(BH.at[0], sem.at[4])
-    await_bytes(SQA.at[pl.ds(0, 3)], sem.at[10])
-    await_bytes(SQC.at[pl.ds(0, 3)], sem.at[6])
-    await_bytes(XR, sem.at[15])
-    await_bytes(ST.at[pl.ds(0, 3)], sem.at[12])
-    for n in (0, 1):
-        for m in range(6):
-            await_bytes(PB.at[0, 0, top], rs_send.at[n, m])
-    await_bytes(PB.at[0, 3], sem.at[8])
-    await_bytes(SQB.at[pl.ds(0, 7)], sem.at[13])
+    await_bytes(HX, own_sem.at[0])
+    await_bytes(HI, own_sem.at[1])
+    await_bytes(CB, own_sem.at[7])
+    await_bytes(BA.at[pl.ds(0, 3)], own_sem.at[8])
+    await_bytes(OW.at[c], own_sem.at[4])
+    await_bytes(RP.at[c], own_sem.at[5])
+    await_bytes(GP.at[c], own_sem.at[6])
+    await_bytes(BH.at[0], own_sem.at[9])
+    await_bytes(SQA.at[pl.ds(0, 3)], own_sem.at[10])
+    await_bytes(SQC.at[pl.ds(0, 3)], own_sem.at[11])
+    await_bytes(XR, own_sem.at[13])
+    await_bytes(ST.at[pl.ds(0, 3)], own_sem.at[12])
+    await_bytes(PB.at[:, pl.ds(0, 3)], own_sem.at[16])
+    await_bytes(PB.at[0, 3], own_sem.at[17])
+    await_bytes(SQB.at[pl.ds(0, 7)], own_sem.at[18])
 
 
 def body(
@@ -616,22 +633,16 @@
             pltpu.VMEM((2, HALF, 256), F32),
             pltpu.VMEM((3, HALF, 256), F32),
             pltpu.VMEM((8, 1, TOK), F32),
-            dma((2, 16)),
-            dma((2, 16)),
+            dma((len(GROUPS),)),
+            dma((len(GROUPS),)),
             dma((2,)),
             dma((2,)),
-            dma((2,)),
-            dma((2,)),
-            dma((2, 2, 2)),
-            dma((2,)),
-            dma((7,)),
+            dma((3, 2)),
+            dma((3, 2)),
             dma((2, 2)),
             dma((2,)),
-            dma((2, 2)),
-            dma((2, 2, 2)),
-            dma((2, 6)),
-            dma((16,)),
             dma((19,)),
+            dma((12,)),
         ],
         compiler_params=pltpu.CompilerParams(
             collective_id=0, has_side_effects=True, vmem_limit_bytes=60 * 1024 * 1024

time: 74.6 us -> 73.5 us (0.985)
  Pallas kernels: 73.7 us -> 72.6 us
    pallas_call x1, Pallas kernels: 73.7 us -> 72.6 us  [body(): pl.pallas_call(layer_kernel, name='layer', out_shape=pltpu.VMEM((2, HALF,...]
where the time goes in v6:
time: 73.5 us; the launch traced here: 73.4 us
  Pallas kernels  72.6 us (99%)
  local copies, waits for them, and re-layouts  0.75 us (1%)
    pallas_call x1, Pallas kernels, body(): pl.pallas_call(layer_kernel, name='layer', out_shape=pltpu.VMEM((2, HALF,...  72.6 us

profile of v6, /device:TPU:1, one launch (start us, length us, event | category | flops | bytes accessed | tf_op | source)
XLA Modules:
  0.0 73.4 jit_solution(8195770265898753931)
XLA Ops:
  0.0 72.6 %layer.1 = bf16[2,384,256]{2,1,0:T(8,128)(2,1)S(1)} custom-call(bf16[768,128]{1,0:T(8,128)(2,1)} %gate_hbm.1, bf16[768,128]{1,0:T(8,128)(2,1)} %rec_hbm.1, s32[6,128]{1,0:T(8,128)} %bitcast.13, bf16[4,128]{1,0:T(4,128)(2,1)} %taps_hbm.1, bf16[2,64,64]{2,1,0:T(8,128)(2,1)} %gmap_hbm.1, bf16[2,64,64]{2,1,0:T(8,128)(2,1)} %imap_hbm.1, f32[1,128]{1,0:T(1,128)} %bitcast.17, ...), custom_call_target="tpu_custom_call" | custom-call | tf_op jit(solution)/shard_map/layer/pallas_call | solution.py:580
  72.6 0.7 %copy.18 = bf16[768,256]{1,0:T(8,128)(2,1)} copy(bf16[768,256]{1,0:T(8,128)(2,1)S(1)} %bitcast.9) | data formatting | bytes 786432

commit v7 on v6

--- a/solution.py
+++ b/solution.py
@@ -113,14 +113,14 @@
     def pass_over(self, ref, where):
         dy = where[1]
         if isinstance(dy, int):
-            late = {0: 0, 1: self.odd, 2: 1, 3: 1 - self.odd}[dy]
+            stage = {0: 0, 1: 1 + self.odd, 2: 2, 3: 2 - self.odd}[dy]
         else:
-            late = 0 if dy is self.mate else 1
+            stage = 1 if dy is self.mate else 2
         pltpu.make_async_remote_copy(
             src_ref=ref,
             dst_ref=ref,
             send_sem=self.pair_send,
-            recv_sem=self.pair_recv.at[late],
+            recv_sem=self.pair_recv.at[stage],
             device_id=(self.slot(0, 0), self.t + 1 - 2 * self.c),
             device_id_type=MESH,
         ).start()
@@ -183,9 +183,9 @@
         if number == 7:
             wait((0, at(0, 1, 2)), (0, at(0, 2, 2)), (1, at(1, 2, 1)), (1, at(1, 2, 2)))
 
-    def wait_pair(self, late):
-        ref = self.buf.at[1 - self.c, pl.ds(0, 8)]
-        pltpu.make_async_copy(ref, ref, self.pair_recv.at[late]).wait()
+    def wait_pair(self, stage):
+        ref = self.buf.at[1 - self.c, pl.ds(0, (4, 4, 8)[stage])]
+        pltpu.make_async_copy(ref, ref, self.pair_recv.at[stage]).wait()
 
     def finish(self):
         ref = self.buf.at[self.c, pl.ds(0, 15)]
@@ -201,7 +201,7 @@
     gate_ref, rec_ref, ids_ref, taps_ref, gmap_ref, imap_ref, level_ref, extra_ref, res_ref,
     mixg_ref, preg_ref, ffng_ref, gw_ref, uw_ref,
     GU, DW, OW, RP, GP, BH, BA, HX, HI, XF, IDF, FA, DV, S, PR, GL, CS, CB, MX, SQA, SO, XR, ST, SQC, SC, ACC, H,
-    PB, RA, RC, PO, FO, FF, PRE, SQB,
+    PB, PS, RA, RC, PO, FO, FL, FF, PRE, LPRE, SQB,
     gu_ring, dw_ring, gu_pair, dw_pair, ba_ring, ag_ring, ra_recv, rc_recv, own_sem, sem,
 ):
     s, t = lax.axis_index("sp"), lax.axis_index("tp")
@@ -456,6 +456,7 @@
         remote(ref, ref, own_sem.at[12], ag_ring.at[2, 0], along_x(step))
     gu.event(6)
     gu.wait_pair(0)
+    gu.wait_pair(1)
     for tile in range(11):
         ACC[tile] = product(x, early, tile)
     gu.event(7)
@@ -464,7 +465,7 @@
     for tile in range(11):
         ACC[tile] = ACC[tile] + product(left, early, tile) + product(right, early, tile)
     dw.event(2)
-    gu.wait_pair(1)
+    gu.wait_pair(2)
     gather_in(range(6))
     dw.event(3)
     gather_in(range(6, 11))
@@ -474,7 +475,8 @@
     hidden(range(6))
     dw.event(4)
     hidden(range(6, 11))
-    dw.event(5)
+    def columns(p, chip, slot):
+        return jnp.dot(H[p], DW[p, 4 * chip + slot], preferred_element_type=F32)
 
     def down_of(p, chip, h):
         weights = jnp.concatenate([DW[p, 4 * chip + 2 * h], DW[p, 4 * chip + 2 * h + 1]], axis=1)
@@ -483,58 +485,103 @@
     def down(chip, h):
         return down_of(c, chip, h) + down_of(1 - c, chip, h)
 
-    def scatter_across(n, h):
-        PB[n, 0] = (PRE[0] + down_of(1 - c, across, h)).astype(BF16)
+    def send_sum(src, dst, semaphore, device):
+        remote(src, dst, own_sem.at[16], semaphore, device)
+
+    odd = lax.rem(y, 2)
+    blocks = ((y, odd), (y + 1 - 2 * odd, 1 - odd))
+    near = ((right, bottom, top), (left, top, bottom))
+
+    def block_own(q):
+        PRE[q] = columns(c, across, blocks[q][0])
+
+    def block_across(q):
+        slot, j = blocks[q]
+        PB[0, 0, j] = (PRE[q] + columns(1 - c, across, slot)).astype(BF16)
         for m, (rows, step) in enumerate(((top, 1), (bottom, 3))):
-            remote(PB.at[n, 0, rows], RA.at[n, m], own_sem.at[16], ra_recv.at[n, m], along_x(step))
-
-    def own_products(h):
+            send_sum(PB.at[0, 0, j, rows], RA.at[0, m, j], ra_recv.at[q, m], along_x(step))
+
+    def block_near(q):
+        slot, j = blocks[q]
+        for m, (chip, rows, _) in enumerate(near):
+            total = columns(c, chip, slot) + columns(1 - c, chip, slot)
+            PB[0, 1 + m, j] = total.astype(BF16)
+            FO[q, m] = total[:QUARTER] if m == 0 else total[QUARTER:]
+            send_sum(PB.at[0, 1 + m, j, rows], RC.at[m, c, j, rows], rc_recv.at[0], (s, 2 * chip + early))
+
+    def block_relay(q):
+        j = blocks[q][1]
+        for m, (chip, _, rows) in enumerate(near):
+            await_bytes(RA.at[0, m, j], ra_recv.at[q, m])
+            PB[0, 1 + m, j, rows] = (FO[q, m] + RA[0, m, j].astype(F32)).astype(BF16)
+            send_sum(PB.at[0, 1 + m, j, rows], RC.at[m, c, j, rows], rc_recv.at[1], (s, 2 * chip + early))
+
+    late = 1 - early
+
+    def late_own():
         for m, chip in enumerate((across, right, left)):
-            PRE[m] = down_of(c, chip, h)
-
-    def scatter_near(n, h):
-        for m, (chip, rows) in enumerate(((right, bottom), (left, top))):
-            total = PRE[1 + m] + down_of(1 - c, chip, h)
-            PB[n, 1 + m] = total.astype(BF16)
-            FO[n, m] = total[:QUARTER] if m == 0 else total[QUARTER:]
-            remote(
-                PB.at[n, 1 + m, rows], RC.at[m, c, rows], own_sem.at[16], rc_recv.at[0],
-                (s, 2 * chip + h),
-            )
-
-    def scatter_relay(n, h):
-        for m, (chip, rows) in enumerate(((right, top), (left, bottom))):
-            await_bytes(RA.at[n, m], ra_recv.at[n, m])
-            PB[n, 1 + m, rows] = (FO[n, m] + RA[n, m].astype(F32)).astype(BF16)
-            remote(
-                PB.at[n, 1 + m, rows], RC.at[m, c, rows], own_sem.at[16], rc_recv.at[1],
-                (s, 2 * chip + h),
-            )
-
-    own_products(early)
+            LPRE[m] = down_of(c, chip, late)
+
+    def late_total(m, chip):
+        return LPRE[m] + down_of(1 - c, chip, late)
+
+    def late_across():
+        total = late_total(0, across)
+        for j in (0, 1):
+            PB[1, 0, j] = total[:, 128 * j : 128 * j + 128].astype(BF16)
+        for m, (rows, step) in enumerate(((top, 1), (bottom, 3))):
+            send_sum(PB.at[1, 0, :, rows], RA.at[1, m], ra_recv.at[2, m], along_x(step))
+
+    def late_near():
+        for m, (chip, rows, _) in enumerate(near):
+            total = late_total(1 + m, chip)
+            FL[m] = total[:QUARTER] if m == 0 else total[QUARTER:]
+            for j in (0, 1):
+                PB[1, 1 + m, j] = total[:, 128 * j : 128 * j + 128].astype(BF16)
+            send_sum(PB.at[1, 1 + m, :, rows], RC.at[m, c, :, rows], rc_recv.at[0], (s, 2 * chip + late))
+
+    def late_relay():
+        for m, (chip, _, rows) in enumerate(near):
+            await_bytes(RA.at[1, m], ra_recv.at[2, m])
+            for j in (0, 1):
+                total = FL[m, :, 128 * j : 128 * j + 128] + RA[1, m, j].astype(F32)
+                PB[1, 1 + m, j, rows] = total.astype(BF16)
+            send_sum(PB.at[1, 1 + m, :, rows], RC.at[m, c, :, rows], rc_recv.at[1], (s, 2 * chip + late))
+
+    block_own(0)
+    dw.event(5)
     dw.wait_pair(0)
-    scatter_across(0, early)
+    block_across(0)
+    block_near(0)
+    block_own(1)
+    dw.wait_pair(1)
+    block_across(1)
     dw.event(6)
-    scatter_near(0, early)
+    block_near(1)
+    block_relay(0)
     dw.event(7)
-    own_products(1 - early)
-    dw.wait_pair(1)
-    scatter_across(1, 1 - early)
-    scatter_relay(0, early)
-    scatter_near(1, 1 - early)
-    PB[0, 3] = down(x, 1 - c).astype(BF16)
-    remote(PB.at[0, 3], PO.at[c], own_sem.at[17], sem.at[8], partner)
-    scatter_relay(1, 1 - early)
+    late_own()
+    dw.wait_pair(2)
+    late_across()
+    block_relay(1)
+    late_near()
+    PS[...] = down(x, 1 - c).astype(BF16)
+    remote(PS, PO.at[c], own_sem.at[17], sem.at[8], partner)
+    late_relay()
     PO[c] = down(x, c).astype(BF16)
     await_bytes(PO.at[1 - c], sem.at[8])
+    def came(m, k, rows):
+        return jnp.concatenate([RC[m, k, 0, rows], RC[m, k, 1, rows]], axis=1)
+
+    head, rest = slice(0, QUARTER), slice(QUARTER, HALF)
     await_bytes(RC.at[0], rc_recv.at[0])
     for k in (0, 1):
-        FF[k, :QUARTER] = PO[k, :QUARTER].astype(F32) + RC[1, k, :QUARTER].astype(F32)
-        FF[k, QUARTER:] = PO[k, QUARTER:].astype(F32) + RC[0, k, QUARTER:].astype(F32)
+        FF[k, head] = PO[k, head].astype(F32) + came(1, k, head).astype(F32)
+        FF[k, rest] = PO[k, rest].astype(F32) + came(0, k, rest).astype(F32)
     await_bytes(RC.at[0], rc_recv.at[1])
     sums = []
     for k in (0, 1):
-        last = jnp.concatenate([RC[0, k, :QUARTER], RC[1, k, QUARTER:]], axis=0)
+        last = jnp.concatenate([came(0, k, head), came(1, k, rest)], axis=0)
         total = (FF[k] + last.astype(F32)).astype(BF16).astype(F32)
         FF[k] = total
         square = jnp.sum(total * total, axis=1, keepdims=True)
@@ -566,8 +613,8 @@
     await_bytes(SQC.at[pl.ds(0, 3)], own_sem.at[11])
     await_bytes(XR, own_sem.at[13])
     await_bytes(ST.at[pl.ds(0, 3)], own_sem.at[12])
-    await_bytes(PB.at[:, pl.ds(0, 3)], own_sem.at[16])
-    await_bytes(PB.at[0, 3], own_sem.at[17])
+    await_bytes(PB, own_sem.at[16])
+    await_bytes(PS, own_sem.at[17])
     await_bytes(SQB.at[pl.ds(0, 7)], own_sem.at[18])
 
 
@@ -625,21 +672,24 @@
             pltpu.VMEM((HALF, 128), F32),
             pltpu.VMEM((11, HALF, 256), F32),
             pltpu.VMEM((2, HALF, HID), BF16),
-            pltpu.VMEM((2, 4, HALF, 256), BF16),
-            pltpu.VMEM((2, 2, HALF // 2, 256), BF16),
-            pltpu.VMEM((2, 2, HALF, 256), BF16),
+            pltpu.VMEM((2, 3, 2, HALF, 128), BF16),
+            pltpu.VMEM((HALF, 256), BF16),
+            pltpu.VMEM((2, 2, 2, HALF // 2, 128), BF16),
+            pltpu.VMEM((2, 2, 2, HALF, 128), BF16),
             pltpu.VMEM((2, HALF, 256), BF16),
-            pltpu.VMEM((2, 2, HALF // 2, 256), F32),
+            pltpu.VMEM((2, 2, HALF // 2, 128), F32),
+            pltpu.VMEM((2, HALF // 2, 256), F32),
             pltpu.VMEM((2, HALF, 256), F32),
+            pltpu.VMEM((2, HALF, 128), F32),
             pltpu.VMEM((3, HALF, 256), F32),
             pltpu.VMEM((8, 1, TOK), F32),
             dma((len(GROUPS),)),
             dma((len(GROUPS),)),
-            dma((2,)),
-            dma((2,)),
+            dma((3,)),
+            dma((3,)),
             dma((3, 2)),
             dma((3, 2)),
-            dma((2, 2)),
+            dma((3, 2)),
             dma((2,)),
             dma((19,)),
             dma((12,)),

time: 73.5 us -> 73.1 us (level)
  no operation moved by 1% of the time
where the time goes in v7:
time: 73.1 us; the launch traced here: 73 us
  Pallas kernels  72.2 us (99%)
  local copies, waits for them, and re-layouts  0.75 us (1%)
    pallas_call x1, Pallas kernels, body(): pl.pallas_call(layer_kernel, name='layer', out_shape=pltpu.VMEM((2, HALF,...  72.2 us

profile of v7, /device:TPU:1, one launch (start us, length us, event | category | flops | bytes accessed | tf_op | source)
XLA Modules:
  0.0 73.0 jit_solution(18440139335662189635)
XLA Ops:
  0.0 72.2 %layer.1 = bf16[2,384,256]{2,1,0:T(8,128)(2,1)S(1)} custom-call(bf16[768,128]{1,0:T(8,128)(2,1)} %gate_hbm.1, bf16[768,128]{1,0:T(8,128)(2,1)} %rec_hbm.1, s32[6,128]{1,0:T(8,128)} %bitcast.13, bf16[4,128]{1,0:T(4,128)(2,1)} %taps_hbm.1, bf16[2,64,64]{2,1,0:T(8,128)(2,1)} %gmap_hbm.1, bf16[2,64,64]{2,1,0:T(8,128)(2,1)} %imap_hbm.1, f32[1,128]{1,0:T(1,128)} %bitcast.17, ...), custom_call_target="tpu_custom_call" | custom-call | tf_op jit(solution)/shard_map/layer/pallas_call | solution.py:627
  72.2 0.7 %copy.18 = bf16[768,256]{1,0:T(8,128)(2,1)} copy(bf16[768,256]{1,0:T(8,128)(2,1)S(1)} %bitcast.9) | data formatting | bytes 786432

commit v8 on v7

--- a/solution.py
+++ b/solution.py
@@ -475,8 +475,9 @@
     hidden(range(6))
     dw.event(4)
     hidden(range(6, 11))
-    def columns(p, chip, slot):
-        return jnp.dot(H[p], DW[p, 4 * chip + slot], preferred_element_type=F32)
+    def columns(p, *slots):
+        weights = jnp.concatenate([DW[p, slot] for slot in slots], axis=1)
+        return jnp.dot(H[p], weights, preferred_element_type=F32)
 
     def down_of(p, chip, h):
         weights = jnp.concatenate([DW[p, 4 * chip + 2 * h], DW[p, 4 * chip + 2 * h + 1]], axis=1)
@@ -493,18 +494,20 @@
     near = ((right, bottom, top), (left, top, bottom))
 
     def block_own(q):
-        PRE[q] = columns(c, across, blocks[q][0])
+        PRE[q] = columns(c, 4 * across + blocks[q][0])
 
     def block_across(q):
         slot, j = blocks[q]
-        PB[0, 0, j] = (PRE[q] + columns(1 - c, across, slot)).astype(BF16)
+        PB[0, 0, j] = (PRE[q] + columns(1 - c, 4 * across + slot)).astype(BF16)
         for m, (rows, step) in enumerate(((top, 1), (bottom, 3))):
             send_sum(PB.at[0, 0, j, rows], RA.at[0, m, j], ra_recv.at[q, m], along_x(step))
 
     def block_near(q):
         slot, j = blocks[q]
+        slots = (4 * right + slot, 4 * left + slot)
+        both = columns(c, *slots) + columns(1 - c, *slots)
         for m, (chip, rows, _) in enumerate(near):
-            total = columns(c, chip, slot) + columns(1 - c, chip, slot)
+            total = both[:, 128 * m : 128 * m + 128]
             PB[0, 1 + m, j] = total.astype(BF16)
             FO[q, m] = total[:QUARTER] if m == 0 else total[QUARTER:]
             send_sum(PB.at[0, 1 + m, j, rows], RC.at[m, c, j, rows], rc_recv.at[0], (s, 2 * chip + early))
@@ -519,22 +522,24 @@
     late = 1 - early
 
     def late_own():
-        for m, chip in enumerate((across, right, left)):
-            LPRE[m] = down_of(c, chip, late)
-
-    def late_total(m, chip):
-        return LPRE[m] + down_of(1 - c, chip, late)
+        LPRE[0] = down_of(c, across, late)
+        both = columns(c, *near_slots)
+        LPRE[1] = both[:, :256]
+        LPRE[2] = both[:, 256:]
+
+    near_slots = [4 * chip + 2 * late + j for chip in (right, left) for j in (0, 1)]
 
     def late_across():
-        total = late_total(0, across)
+        total = LPRE[0] + down_of(1 - c, across, late)
         for j in (0, 1):
             PB[1, 0, j] = total[:, 128 * j : 128 * j + 128].astype(BF16)
         for m, (rows, step) in enumerate(((top, 1), (bottom, 3))):
             send_sum(PB.at[1, 0, :, rows], RA.at[1, m], ra_recv.at[2, m], along_x(step))
 
     def late_near():
+        both = columns(1 - c, *near_slots)
         for m, (chip, rows, _) in enumerate(near):
-            total = late_total(1 + m, chip)
+            total = LPRE[1 + m] + both[:, 256 * m : 256 * m + 256]
             FL[m] = total[:QUARTER] if m == 0 else total[QUARTER:]
             for j in (0, 1):
                 PB[1, 1 + m, j] = total[:, 128 * j : 128 * j + 128].astype(BF16)
@@ -558,8 +563,8 @@
     block_across(1)
     dw.event(6)
     block_near(1)
+    dw.event(7)
     block_relay(0)
-    dw.event(7)
     late_own()
     dw.wait_pair(2)
     late_across()

time: 73.1 us -> 72.6 us (level)
  no operation moved by 1% of the time
where the time goes in v8:
time: 72.6 us; the launch traced here: 72.5 us
  Pallas kernels  71.7 us (99%)
  local copies, waits for them, and re-layouts  0.75 us (1%)
    pallas_call x1, Pallas kernels, body(): pl.pallas_call(layer_kernel, name='layer', out_shape=pltpu.VMEM((2, HALF,...  71.7 us

profile of v8, /device:TPU:1, one launch (start us, length us, event | category | flops | bytes accessed | tf_op | source)
XLA Modules:
  0.0 72.5 jit_solution(1803616412155656798)
XLA Ops:
  0.0 71.7 %layer.1 = bf16[2,384,256]{2,1,0:T(8,128)(2,1)S(1)} custom-call(bf16[768,128]{1,0:T(8,128)(2,1)} %gate_hbm.1, bf16[768,128]{1,0:T(8,128)(2,1)} %rec_hbm.1, s32[6,128]{1,0:T(8,128)} %bitcast.13, bf16[4,128]{1,0:T(4,128)(2,1)} %taps_hbm.1, bf16[2,64,64]{2,1,0:T(8,128)(2,1)} %gmap_hbm.1, bf16[2,64,64]{2,1,0:T(8,128)(2,1)} %imap_hbm.1, f32[1,128]{1,0:T(1,128)} %bitcast.17, ...), custom_call_target="tpu_custom_call" | custom-call | tf_op jit(solution)/shard_map/layer/pallas_call | solution.py:632
  71.7 0.7 %copy.18 = bf16[768,256]{1,0:T(8,128)(2,1)} copy(bf16[768,256]{1,0:T(8,128)(2,1)S(1)} %bitcast.9) | data formatting | bytes 786432

commit v9 on v8

--- a/solution.py
+++ b/solution.py
@@ -253,11 +253,6 @@
     GU[c, own, :, 1280:1408] = block.T.astype(BF16)
     for load in loads[2:4]:
         load.wait()
-    IDF[8:] = jnp.concatenate(
-        [jnp.broadcast_to(ids_ref[r : r + 1, :].astype(F32), (128, 128)).T for r in range(6)], axis=0
-    )
-    XF[8:] = rec_ref[...].astype(F32)
-
     pl.semaphore_wait(barrier, 2 * REACH + 7)
 
     after = (lax.rem(s + 1, 16), t)
@@ -273,6 +268,11 @@
     remote(OW.at[c], OW.at[c], own_sem.at[4], sem.at[9], partner)
     remote(res_ref.at[1 - c], RP.at[c], own_sem.at[5], sem.at[10], partner)
     remote(GP.at[c], GP.at[c], own_sem.at[6], sem.at[11], partner)
+
+    IDF[8:] = jnp.concatenate(
+        [jnp.broadcast_to(ids_ref[r : r + 1, :].astype(F32), (128, 128)).T for r in range(6)], axis=0
+    )
+    XF[8:] = rec_ref[...].astype(F32)
 
     for r in range(6):
         rows = slice(128 * r, 128 * r + 128)
@@ -564,8 +564,8 @@
     dw.event(6)
     block_near(1)
     dw.event(7)
+    late_own()
     block_relay(0)
-    late_own()
     dw.wait_pair(2)
     late_across()
     block_relay(1)

time: 72.6 us -> 72.5 us (level)
  no operation moved by 1% of the time
where the time goes in v9:
time: 72.5 us; the launch traced here: 72.4 us
  Pallas kernels  71.7 us (99%)
  local copies, waits for them, and re-layouts  0.75 us (1%)
    pallas_call x1, Pallas kernels, body(): pl.pallas_call(layer_kernel, name='layer', out_shape=pltpu.VMEM((2, HALF,...  71.7 us

profile of v9, /device:TPU:1, one launch (start us, length us, event | category | flops | bytes accessed | tf_op | source)
XLA Modules:
  0.0 72.4 jit_solution(4495183375631261149)
XLA Ops:
  0.0 71.7 %layer.1 = bf16[2,384,256]{2,1,0:T(8,128)(2,1)S(1)} custom-call(bf16[768,128]{1,0:T(8,128)(2,1)} %gate_hbm.1, bf16[768,128]{1,0:T(8,128)(2,1)} %rec_hbm.1, s32[6,128]{1,0:T(8,128)} %bitcast.13, bf16[4,128]{1,0:T(4,128)(2,1)} %taps_hbm.1, bf16[2,64,64]{2,1,0:T(8,128)(2,1)} %gmap_hbm.1, bf16[2,64,64]{2,1,0:T(8,128)(2,1)} %imap_hbm.1, f32[1,128]{1,0:T(1,128)} %bitcast.17, ...), custom_call_target="tpu_custom_call" | custom-call | tf_op jit(solution)/shard_map/layer/pallas_call | solution.py:632
  71.7 0.7 %copy.18 = bf16[768,256]{1,0:T(8,128)(2,1)} copy(bf16[768,256]{1,0:T(8,128)(2,1)S(1)} %bitcast.9) | data formatting | bytes 786432
